TPU v7x, 256 devices: a whole 4x4x8 slice. The times are simulated.
256 devices in a mesh: sp: 32 (over z, y), dp: 8 (over x, core).
Axes of the slice: x: 4, y: 4, z: 8, core: 2. Of those that a mesh axis runs over, the one named last changes fastest.
Arguments:
- cotangent: bfloat16 [8, 8192, 4096], P('dp', 'sp'), may hold values from -6 to 6
- up_pre: bfloat16 [8, 8192, 4096], P('dp', 'sp'), may hold values from -6 to 6
- value_pre: bfloat16 [8, 8192, 4096], P('dp', 'sp'), may hold values from -6 to 6
- spatial_weight: bfloat16 [32, 1024, 1024], P('sp', 'dp'), may hold values from -0.1875 to 0.1875
- spatial_bias: float32 [32, 1024], P('sp'), may hold values from 0.5 to 1.5
- value_gain: float32 [4096], replicated, may hold values from 0.1 to 1.9
Outputs:
- up_grad: bfloat16 [8, 8192, 4096], P('dp', 'sp')
- value_grad: bfloat16 [8, 8192, 4096], P('dp', 'sp')
- weight_grad: float32 [32, 1024, 1024], P('sp', 'dp')
- bias_grad: float32 [32, 1024], P('sp', 'dp')
- gain_grad: float32 [4096], replicated
All inputs are finite; a program needn't handle non-finite values.
Results may differ from a plain program's by a relative error of at most 0.0064.
Values may be sent and summed in bfloat16 or wider, within the bound.
A program may use at most 128 MiB of HBM per device.

v0:
```python
import functools
import math

import jax
import jax.numpy as jnp
from jax import lax
from jax.sharding import Mesh
from jax.sharding import PartitionSpec as P

SP = ("sp_0", "sp_1")
DP = ("dp_0", "dp_1")
SP_DP = ("sp_0", "sp_1", "dp_0", "dp_1")


norm_floor = 0.5
root_half = 1.0 / math.sqrt(2.0)
inv_root_tau = 1.0 / math.sqrt(2.0 * math.pi)


def joined_along(blocks, dim):
    blocks = jnp.moveaxis(blocks, 0, dim)
    shape = blocks.shape
    return blocks.reshape(*shape[:dim], shape[dim] * shape[dim + 1], *shape[dim + 2 :])


def from_everyone(shard, axis):
    copies = jnp.broadcast_to(shard, (lax.axis_size(axis), *shard.shape))
    return lax.all_to_all(copies, axis, split_axis=0, concat_axis=0, tiled=True)


def gathered_copies(shard, axis, dim):
    return joined_along(from_everyone(shard, axis), dim)


def in_one_piece(arrays, axis, dim, along):
    columns = [a.reshape(*a.shape[:along], -1) for a in arrays]
    both = jnp.concatenate(columns, axis=along)
    result, at, done = (lax.psum_scatter(both, axis, scatter_dimension=dim, tiled=True), 0, [])
    for a, column in zip(arrays, columns):
        slab = result[..., at : at + column.shape[along]]
        done.append(slab.reshape(*slab.shape[:along], *a.shape[along:]))
        at += column.shape[along]
    return tuple(done)


def sent_together(arrays, axis, split_dim, concat_dim, along):
    widths = [a.shape[along] for a in arrays]
    both = jnp.concatenate(arrays, axis=along)
    result = lax.all_to_all(both, axis, split_axis=split_dim, concat_axis=concat_dim, tiled=True)
    return tuple(jnp.split(result, [sum(widths[:k]) for k in range(1, len(widths))], axis=along))


def by_axis(shard, axes):
    return functools.reduce(lax.psum, axes, shard)


def gelu_slope(values):
    return (
        0.5 * (1.0 + jax.scipy.special.erf(values * root_half))
        + values * jnp.exp(-0.5 * values * values) * inv_root_tau
    )


def shards(cotangent, up_pre, value_pre, spatial_weight, spatial_bias, value_gain):
    tok_rows = cotangent.shape[1]
    model_width = cotangent.shape[2]
    grp_dev = spatial_weight.shape[0]
    block_len = spatial_weight.shape[2]
    sp_count = lax.axis_size(SP)
    all_groups = grp_dev * sp_count
    group_dim = model_width // all_groups
    seq_len = tok_rows * sp_count
    blocks = seq_len // block_len
    grad_tok = cotangent[0].astype(jnp.float32)
    up_arg = up_pre[0].astype(jnp.float32)
    value_arg = value_pre[0].astype(jnp.float32)
    up_act = lax.optimization_barrier(jax.nn.gelu(up_arg, approximate=False).astype(jnp.bfloat16))
    value_act = jax.nn.gelu(value_arg, approximate=False)
    inv_rms = lax.rsqrt(jnp.mean(value_act * value_act, axis=-1, keepdims=True) + norm_floor)
    normed = value_act * inv_rms
    value_norm = (normed * value_gain).astype(jnp.bfloat16)
    split_shape = (tok_rows, all_groups, group_dim)
    gate_tok = (grad_tok * up_act.astype(jnp.float32)).astype(jnp.bfloat16)
    gate_heads, value_heads = (
        lax.all_to_all(gate_tok.reshape(split_shape), SP, split_axis=1, concat_axis=0, tiled=True),
        lax.all_to_all(
            value_norm.reshape(split_shape), SP, split_axis=1, concat_axis=0, tiled=True
        ),
    )
    block_shape = (blocks, block_len, grp_dev, group_dim)
    gate_blocks = gate_heads.reshape(block_shape)
    value_blocks = value_heads.reshape(block_shape)
    portion = gathered_copies(spatial_weight, DP, 1)
    mixed_rows = jnp.einsum(
        "gpq,nqgc->npgc", portion, value_blocks, preferred_element_type=jnp.float32
    )
    mixed_acc = mixed_rows
    back_acc = jnp.einsum(
        "gpq,npgc->nqgc", portion, gate_blocks, preferred_element_type=jnp.float32
    )
    mixed_acc, back_acc = (mixed_acc, back_acc)
    mixed_out = lax.optimization_barrier(
        (mixed_acc + spatial_bias.T[None, :, :, None]).astype(jnp.bfloat16)
    )
    back_heads = back_acc.astype(jnp.bfloat16)
    weight_term = jnp.einsum(
        "npgc,nqgc->gpq", gate_blocks, value_blocks, preferred_element_type=jnp.float32
    )
    bias_term = jnp.sum(gate_blocks, axis=(0, 3), dtype=jnp.float32).T
    weight_grad, bias_grad = in_one_piece((weight_term, bias_term), DP, 1, 2)
    heads_shape = (seq_len, grp_dev, group_dim)
    first_heads = mixed_out.reshape(heads_shape)
    first_tok, back_tok = sent_together((first_heads, back_heads.reshape(heads_shape)), SP, 0, 1, 2)
    up_mid = lax.optimization_barrier(
        (grad_tok * first_tok.reshape(tok_rows, model_width).astype(jnp.float32)).astype(
            jnp.bfloat16
        )
    )
    up_grad = (up_mid.astype(jnp.float32) * gelu_slope(up_arg)).astype(jnp.bfloat16)[None]
    back_full = back_tok.reshape(tok_rows, model_width).astype(jnp.float32)
    gain_grad = by_axis(jnp.sum(back_full * normed, axis=0), SP_DP)
    scaled = back_full * value_gain
    value_slope = inv_rms * scaled - inv_rms**3 * value_act * jnp.mean(
        scaled * value_act, axis=-1, keepdims=True
    )
    value_grad = (value_slope * gelu_slope(value_arg)).astype(jnp.bfloat16)[None]
    return (up_grad, value_grad, weight_grad, bias_grad, gain_grad)


def solution(mesh):
    torus = Mesh(mesh.devices.reshape(8, 4, 4, 2), ("sp_0", "sp_1", "dp_0", "dp_1"))
    in_specs = (
        P(DP, SP, None),
        P(DP, SP, None),
        P(DP, SP, None),
        P(SP, DP, None),
        P(SP, None),
        P(),
    )
    out_specs = (P(DP, SP, None), P(DP, SP, None), P(SP, DP, None), P(SP, DP), P())
    return jax.shard_map(
        shards, mesh=torus, in_specs=in_specs, out_specs=out_specs, check_vma=False
    )
```

profile of v0, /device:TPU:33, one launch (start us, length us, event | category | flops | bytes accessed | tf_op | source)
XLA Modules:
  0.0 438.5 jit_solution(10742665178344789631)
XLA Ops:
  9.7 5.0 %all-to-all-start.1 = ((bf16[8,1,128,1024]{3,2,1,0:T(8,128)(2,1)}), bf16[8,1,128,1024]{3,2,1,0:T(8,128)(2,1)}, u32[]{:S(2)}, u32[]{:S(2)}) async-start(bf16[8,1,128,1024]{3,2,1,0:T(8,128)(2,1)} %broadcast_in_dim.4), calls=%async_computation.1 | async-start | bytes 4194304 | tf_op jit(solution)/shard_map/all_to_all | solution.py:28
  17.9 9.4 %fusion.7 = f32[256]{0:T(256)S(1)} fusion(bf16[1,256,4096]{1,2,0:T(8,128)(2,1)S(1)} %copy.47), kind=kLoop, calls=%fused_computation.26 | loop fusion | flops 70254336 | bytes 2098176 | tf_op jit(solution)/shard_map/reduce_sum | solution.py:79
  31.4 10.9 %fusion.10 = bf16[256,4096]{0,1:T(8,128)(2,1)} fusion(bf16[1,256,4096]{1,2,0:T(8,128)(2,1)} %copy.51), kind=kLoop, calls=%fused_computation.29 | loop fusion | flops 69206016 | bytes 4194304 | tf_op jit(solution)/shard_map/convert_element_type | solution.py:77
  50.5 10.9 %all-to-all-start.2 = ((bf16[256,32,128]{0,2,1:T(8,128)(2,1)}), bf16[256,32,128]{0,2,1:T(8,128)(2,1)}, u32[]{:S(2)}, u32[]{:S(2)}) async-start(bf16[256,32,128]{0,2,1:T(8,128)(2,1)} %bitcast.156), calls=%async_computation.2 | async-start | bytes 4194304 | tf_op jit(solution)/shard_map/all_to_all | solution.py:85
  62.1 10.0 %multiply_convert_fusion = (bf16[256,32,128]{0,2,1:T(8,128)(2,1)}, f32[256,32,128]{0,2,1:T(8,128)}) fusion(f32[32,128]{1,0:T(8,128)S(1)} %bitcast.164, f32[256]{0:T(256)S(1)} %get-tuple-element.39, f32[256,32,128]{0,2,1:T(8,128)S(1)} %bitcast.154, f32[256,32,128]{0,2,1:T(8,128)S(1)} %bitcast.153), kind=kLoop, calls=%fused_computation.141 | loop fusion | flops 67108864 | bytes 14697472 | tf_op jit(solution)/shard_map/convert_element_type | solution.py:81
  72.1 38.7 %all-to-all-done.2 = bf16[256,32,128]{0,2,1:T(8,128)(2,1)} async-done(((bf16[256,32,128]{0,2,1:T(8,128)(2,1)}), bf16[256,32,128]{0,2,1:T(8,128)(2,1)}, u32[]{:S(2)}, u32[]{:S(2)}) %all-to-all-start.2) | async-done | bytes 2097184 | tf_op jit(solution)/shard_map/all_to_all | solution.py:85
  110.8 6.4 %all-to-all-start = ((bf16[256,32,128]{0,2,1:T(8,128)(2,1)}), bf16[256,32,128]{0,2,1:T(8,128)(2,1)}, u32[]{:S(2)}, u32[]{:S(2)}) async-start(bf16[256,32,128]{0,2,1:T(8,128)(2,1)} %get-tuple-element.32), calls=%async_computation | async-start | bytes 4194304 | tf_op jit(solution)/shard_map/all_to_all | solution.py:86
  121.3 5.9 %convert_bitcast_fusion = bf16[8,1024,1,128]{1,3,0,2:T(8,128)(2,1)} fusion(bf16[8,1024,128]{2,1,0:T(8,128)(2,1)} %bitcast.159, bf16[1024,1024,1]{1,0,2:T(8,128)(2,1)} %bitcast.11), kind=kOutput, calls=%fused_computation.158 | convolution fusion | flops 2148532224 | bytes 6291456 | tf_op jit(solution)/shard_map/gpq,npgc->nqgc/dot_general | solution.py:98
  131.1 33.4 %all-to-all-done = bf16[256,32,128]{0,2,1:T(8,128)(2,1)} async-done(((bf16[256,32,128]{0,2,1:T(8,128)(2,1)}), bf16[256,32,128]{0,2,1:T(8,128)(2,1)}, u32[]{:S(2)}, u32[]{:S(2)}) %all-to-all-start) | async-done | bytes 2097184 | tf_op jit(solution)/shard_map/all_to_all | solution.py:86
  168.5 6.0 %fusion.120 = bf16[8,1024,1,128]{1,3,0,2:T(8,128)(2,1)} fusion(f32[1024]{0:T(1024)S(1)} %bitcast.168, bf16[8,1024,128]{2,1,0:T(8,128)(2,1)} %bitcast.161, bf16[1024,1024,1]{1,0,2:T(8,128)(2,1)} %bitcast.11), kind=kOutput, calls=%fused_computation.160 | convolution fusion | flops 2149580800 | bytes 6295552 | tf_op jit(solution)/shard_map/gpq,nqgc->npgc/dot_general | solution.py:94
  178.4 4.6 %pad_maximum_fusion.1 = bf16[8192,1,256]{2,0,1:T(8,128)(2,1)} fusion(bf16[8192,1,128]{2,0,1:T(8,128)(2,1)} %bitcast.157, bf16[8192,1,128]{2,0,1:T(8,128)(2,1)} %bitcast.158), kind=kLoop, calls=%fused_computation.79 | loop fusion | flops 8388608 | bytes 8388608 | tf_op jit(solution)/shard_map/concatenate | solution.py:48
  183.5 6.7 %reduce.6 = bf16[8192,256]{1,0:T(8,128)(2,1)} reduce(bf16[8192,1,256]{2,0,1:T(8,128)(2,1)} %pad_maximum_fusion.1, bf16[]{:T(256)} %broadcast.719), dimensions={1}, to_apply=%copy.55.reduce_sub_computation | reduce | bytes 8388610 | tf_op jit(solution)/shard_map/concatenate | solution.py:48
  190.2 6.9 %reshape.207 = bf16[32,2,32768]{2,1,0:T(2,128)(2,1)} reshape(bf16[8192,256]{1,0:T(8,128)(2,1)} %reduce.6) | data formatting | bytes 8388608
  197.1 7.5 %all-to-all-start.3 = ((bf16[32,2,32768]{2,1,0:T(2,128)(2,1)}), bf16[32,2,32768]{2,1,0:T(2,128)(2,1)}, u32[]{:S(2)}, u32[]{:S(2)}) async-start(bf16[32,2,32768]{2,1,0:T(2,128)(2,1)} %reshape.207), calls=%async_computation.3 | async-start | bytes 8388608 | tf_op jit(solution)/shard_map/all_to_all | solution.py:49
  206.9 4.6 %convolution_bitcast_fusion = f32[1,1024,1024]{1,2,0:T(8,128)S(1)} fusion(bf16[8,1024,128]{2,1,0:T(8,128)(2,1)} %bitcast.160, bf16[8,1024,128]{2,1,0:T(8,128)(2,1)} %bitcast.162), kind=kOutput, calls=%fused_computation.156 | convolution fusion | flops 2147483648 | bytes 8388608 | tf_op jit(solution)/shard_map/npgc,nqgc->gpq/dot_general | solution.py:106
  213.8 81.5 %all-to-all-done.3 = bf16[32,2,32768]{2,1,0:T(2,128)(2,1)} async-done(((bf16[32,2,32768]{2,1,0:T(2,128)(2,1)}), bf16[32,2,32768]{2,1,0:T(2,128)(2,1)}, u32[]{:S(2)}, u32[]{:S(2)}) %all-to-all-start.3) | async-done | bytes 4194336 | tf_op jit(solution)/shard_map/all_to_all | solution.py:49
  295.3 19.8 %reshape.208 = bf16[8192,1,256]{2,1,0:T(2,128)(2,1)} reshape(bf16[32,2,32768]{2,1,0:T(2,128)(2,1)} %all-to-all-done.3) | data formatting | bytes 8388608
  315.1 6.0 %copy.62 = bf16[8192,1,256]{2,0,1:T(8,128)(2,1)} copy(bf16[8192,1,256]{2,1,0:T(2,128)(2,1)} %reshape.208) | data formatting | bytes 8388608
  321.2 6.4 %copy.56 = bf16[32,256,1,256]{1,3,0,2:T(8,128)(2,1)} copy(bf16[32,256,1,256]{3,1,0,2:T(8,128)(2,1)} %bitcast.155) | data formatting | bytes 8388608 | tf_op jit(solution)/shard_map/all_to_all | solution.py:49
  333.7 14.7 %fusion.17 = bf16[1,256,4096]{1,2,0:T(8,128)(2,1)} fusion(bf16[1,256,4096]{1,2,0:T(8,128)(2,1)S(1)} %copy.47, f32[256,32,128]{0,2,1:T(8,128)S(1)} %get-tuple-element.34, f32[256]{0:T(256)S(1)} %broadcast_multiply_fusion, f32[256]{0:T(256)S(1)} %get-tuple-element.38, f32[4096]{0:T(1024)S(1)} %copy-done.3, f32[256]{0:T(256)S(1)} %get-tuple-element.39), kind=kLoop, calls=%fused_computation.36 | loop fusion | flops 83886080 | bytes 8408064 | tf_op jit(solution)/shard_map/convert_element_type | solution.py:126
  359.9 21.1 %psum.28 = f32[4096]{0:T(1024)S(1)} all-reduce(f32[4096]{0:T(1024)S(1)} %bitcast.166), channel_id=1, replica_groups=mesh['sp_0'=8,'sp_1'=4,'dp_0'=4,'dp_1'=2] {'sp_0'}, use_global_device_ids=true, to_apply=%region_6.0 | all-reduce | flops 4096 | bytes 32768 | tf_op jit(solution)/shard_map/psum | solution.py:54
  380.9 15.4 %psum.29 = f32[4096]{0:T(1024)S(1)} all-reduce(f32[4096]{0:T(1024)S(1)} %psum.28), channel_id=1, replica_groups=mesh['sp_0'=8,'sp_1'=4,'dp_0'=4,'dp_1'=2] {'sp_1'}, use_global_device_ids=true, to_apply=%region_7.0 | all-reduce | flops 4096 | bytes 32768 | tf_op jit(solution)/shard_map/psum | solution.py:54
  396.3 13.1 %psum.30 = f32[4096]{0:T(1024)S(1)} all-reduce(f32[4096]{0:T(1024)S(1)} %psum.29), channel_id=1, replica_groups=mesh['sp_0'=8,'sp_1'=4,'dp_0'=4,'dp_1'=2] {'dp_0'}, use_global_device_ids=true, to_apply=%region_8.0 | all-reduce | flops 4096 | bytes 32768 | tf_op jit(solution)/shard_map/psum | solution.py:54
  409.4 19.0 %psum.31 = f32[4096]{0:T(1024)} all-reduce(f32[4096]{0:T(1024)S(1)} %psum.30), channel_id=1, replica_groups=mesh['sp_0'=8,'sp_1'=4,'dp_0'=4,'dp_1'=2] {'dp_1'}, use_global_device_ids=true, to_apply=%region_9.10 | all-reduce | flops 4096 | bytes 32768 | tf_op jit(solution)/shard_map/psum | solution.py:54
  (40 shorter events, 60.6 us)
Async XLA Ops:
  9.7 40.8 %all-to-all-start.1 = ((bf16[8,1,128,1024]{3,2,1,0:T(8,128)(2,1)}), bf16[8,1,128,1024]{3,2,1,0:T(8,128)(2,1)}, u32[]{:S(2)}, u32[]{:S(2)}) async-start(bf16[8,1,128,1024]{3,2,1,0:T(8,128)(2,1)} %broadcast_in_dim.4), calls=%async_computation.1 | async-start | bytes 4194304 | tf_op jit(solution)/shard_map/all_to_all | solution.py:28
  50.5 60.3 %all-to-all-start.2 = ((bf16[256,32,128]{0,2,1:T(8,128)(2,1)}), bf16[256,32,128]{0,2,1:T(8,128)(2,1)}, u32[]{:S(2)}, u32[]{:S(2)}) async-start(bf16[256,32,128]{0,2,1:T(8,128)(2,1)} %bitcast.156), calls=%async_computation.2 | async-start | bytes 4194304 | tf_op jit(solution)/shard_map/all_to_all | solution.py:85
  61.3 0.7 copy-start.3
  110.8 53.7 %all-to-all-start = ((bf16[256,32,128]{0,2,1:T(8,128)(2,1)}), bf16[256,32,128]{0,2,1:T(8,128)(2,1)}, u32[]{:S(2)}, u32[]{:S(2)}) async-start(bf16[256,32,128]{0,2,1:T(8,128)(2,1)} %get-tuple-element.32), calls=%async_computation | async-start | bytes 4194304 | tf_op jit(solution)/shard_map/all_to_all | solution.py:86
  127.1 41.4 %copy-start.4 = (f32[1,1024]{1,0:T(1,128)S(1)}, f32[1,1024]{1,0:T(1,128)}, u32[]{:S(2)}) copy-start(f32[1,1024]{1,0:T(1,128)} %param.10) | copy-start | bytes 12292
  197.1 98.2 %all-to-all-start.3 = ((bf16[32,2,32768]{2,1,0:T(2,128)(2,1)}), bf16[32,2,32768]{2,1,0:T(2,128)(2,1)}, u32[]{:S(2)}, u32[]{:S(2)}) async-start(bf16[32,2,32768]{2,1,0:T(2,128)(2,1)} %reshape.207), calls=%async_computation.3 | async-start | bytes 8388608 | tf_op jit(solution)/shard_map/all_to_all | solution.py:49
  204.6 223.7 %reduce-scatter.2.cloned.1.call-start = ((), (), s32[]{:S(2)}) async-start(), calls=%async_computation.5 | async-start | bytes 4755456 | tf_op jit(solution)/shard_map/reduce_scatter | solution.py:38
  327.6 4.1 copy-start
  348.4 4.2 copy-start.1
  352.7 2.3 copy-start.2
Sparse Core Ops, SparseCore 0:
  213.9 41.3 reduce-scatter.1
where the time goes:
time: 444 us; the launch traced here: 438 us
  waiting for transfers between devices  154 us (35%)
  local copies, waits for them, and re-layouts  80.4 us (18%)
  other arithmetic  75.4 us (17%)
  blocking collectives  68.5 us (15%)
  starting transfers between devices  30 us (7%)
  matrix products  16.4 us (4%)
  between operations  14.2 us (3%)
    all_to_all x1, waiting for transfers between devices, sent_together(): lax.all_to_all(both, axis, split_axis=split_dim, concat_axis=concat_dim,...  81.5 us
    psum x4, blocking collectives, by_axis(): return functools.reduce(lax.psum, axes, shard)  68.5 us
    unnamed x19, local copies, waits for them, and re-layouts  52.7 us
    all_to_all x1, waiting for transfers between devices, shards(): lax.all_to_all(gate_tok.reshape(split_shape), SP, split_axis=1, concat_ax...  38.7 us
    all_to_all x1, waiting for transfers between devices, shards(): lax.all_to_all(value_norm.reshape(split_shape), SP, split_axis=1, concat_...  33.4 us
    convert_element_type x1, other arithmetic, shards(): (value_slope * gelu_slope(value_arg)).astype(jnp.bfloat16)[None]  14.7 us
    concatenate x2, other arithmetic, sent_together(): both = jnp.concatenate(arrays, axis=along)  11.3 us
    convert_element_type x1, other arithmetic, shards(): jax.nn.gelu(up_arg, approximate=False).astype(jnp.bfloat16)  10.9 us
  transfers between devices with their start and end apart: 5, of which 3 were waited for; matrix products, arithmetic and copies ran while one was open for 30% of the time, Pallas kernels for 0%

commit v1 on v0

v1 whole, which is shorter than its diff:
```python
import math

import jax
import jax.numpy as jnp
from jax import lax
from jax.sharding import Mesh
from jax.sharding import PartitionSpec as P

SP = ("sp_0", "sp_1")
DP = ("dp_0", "dp_1")
PLANE = ("dp_0", "dp_1", "sp_1")
SWAP = ("sp_0", "dp_0", "dp_1")
ALL = ("sp_0", "sp_1", "dp_0", "dp_1")


norm_floor = 0.5
root_half = 1.0 / math.sqrt(2.0)
inv_root_tau = 1.0 / math.sqrt(2.0 * math.pi)


def gelu_slope(values):
    return (
        0.5 * (1.0 + jax.scipy.special.erf(values * root_half))
        + values * jnp.exp(-0.5 * values * values) * inv_root_tau
    )


def swapped(shard, n):
    pairs = [(a * n + b, b * n + a) for a in range(n) for b in range(n)]
    return lax.ppermute(shard, SWAP, pairs)


def shards(cotangent, up_pre, value_pre, spatial_weight, spatial_bias, value_gain):
    rows, width = cotangent.shape[1:]
    block_len = spatial_weight.shape[2]
    planes = lax.axis_size("sp_0")
    seqs = lax.axis_size(DP)
    groups = lax.axis_size(PLANE)
    dim = width // groups
    weight = lax.all_gather(swapped(spatial_weight[0], planes), "sp_0", axis=0, tiled=True)
    bias = swapped(spatial_bias, planes)[0]

    grad_tok = cotangent[0].astype(jnp.float32)
    up_arg = up_pre[0].astype(jnp.float32)
    value_arg = value_pre[0].astype(jnp.float32)
    up_act = lax.optimization_barrier(jax.nn.gelu(up_arg, approximate=False).astype(jnp.bfloat16))
    value_act = jax.nn.gelu(value_arg, approximate=False)
    inv_rms = lax.rsqrt(jnp.mean(value_act * value_act, axis=-1, keepdims=True) + norm_floor)
    normed = value_act * inv_rms
    value_norm = (normed * value_gain).astype(jnp.bfloat16)
    gate_tok = (grad_tok * up_act.astype(jnp.float32)).astype(jnp.bfloat16)

    def outward(tok):
        tok = tok.reshape(rows, groups, dim).transpose(1, 0, 2)
        got = lax.all_to_all(tok, PLANE, split_axis=0, concat_axis=0, tiled=True)
        return got.reshape(seqs, block_len, dim)

    def homeward(heads):
        got = heads.reshape(groups, rows, dim)
        got = lax.all_to_all(got, PLANE, split_axis=0, concat_axis=0, tiled=True)
        return got.transpose(1, 0, 2).reshape(rows, width)

    value_blocks = outward(value_norm)
    gate_blocks = outward(gate_tok)
    back_heads = jnp.einsum(
        "pq,npc->nqc", weight, gate_blocks, preferred_element_type=jnp.float32
    ).astype(jnp.bfloat16)
    back_full = homeward(back_heads).astype(jnp.float32)
    mixed_heads = jnp.einsum("pq,nqc->npc", weight, value_blocks, preferred_element_type=jnp.float32)
    mixed_heads = (mixed_heads + bias[None, :, None]).astype(jnp.bfloat16)
    mixed_tok = homeward(mixed_heads).astype(jnp.float32)
    weight_term = jnp.einsum(
        "npc,nqc->pq", gate_blocks, value_blocks, preferred_element_type=jnp.float32
    )
    bias_term = jnp.sum(gate_blocks, axis=(0, 2), dtype=jnp.float32)
    both = jnp.concatenate([weight_term, jnp.broadcast_to(bias_term[:, None], (block_len, 128))], axis=1)
    both = lax.psum_scatter(both, "sp_0", scatter_dimension=0, tiled=True)
    both = swapped(both, planes)
    weight_grad = both[None, :, :block_len]
    bias_grad = both[None, :, block_len]

    up_mid = lax.optimization_barrier((grad_tok * mixed_tok).astype(jnp.bfloat16))
    up_grad = (up_mid.astype(jnp.float32) * gelu_slope(up_arg)).astype(jnp.bfloat16)[None]
    gain_grad = lax.psum(jnp.sum(back_full * normed, axis=0), ALL)
    scaled = back_full * value_gain
    value_slope = inv_rms * scaled - inv_rms**3 * value_act * jnp.mean(
        scaled * value_act, axis=-1, keepdims=True
    )
    value_grad = (value_slope * gelu_slope(value_arg)).astype(jnp.bfloat16)[None]
    return (up_grad, value_grad, weight_grad, bias_grad, gain_grad)


def solution(mesh):
    torus = Mesh(mesh.devices.reshape(8, 4, 4, 2), ("sp_0", "sp_1", "dp_0", "dp_1"))
    in_specs = (
        P(DP, SP, None),
        P(DP, SP, None),
        P(DP, SP, None),
        P(SP, DP, None),
        P(SP, None),
        P(),
    )
    out_specs = (P(DP, SP, None), P(DP, SP, None), P(SP, DP, None), P(SP, DP), P())
    return jax.shard_map(
        shards, mesh=torus, in_specs=in_specs, out_specs=out_specs, check_vma=False
    )
```

time: 444 us -> 387 us (0.87)
  the two profiles are of different devices: /device:TPU:33 before, /device:TPU:47 now
where the time goes in v1:
time: 387 us; the launch traced here: 386 us
  waiting for transfers between devices  108 us (28%)
  other arithmetic  77.7 us (20%)
  blocking collectives  76.8 us (20%)
  local copies, waits for them, and re-layouts  47.5 us (12%)
  starting transfers between devices  47.3 us (12%)
  matrix products  14.2 us (4%)
  between operations  14.2 us (4%)
    psum x1, blocking collectives, shards(): gain_grad = lax.psum(jnp.sum(back_full * normed, axis=0), ALL)  76.8 us
    ppermute x3, waiting for transfers between devices, swapped(): return lax.ppermute(shard, SWAP, pairs)  48.7 us
    all_to_all x2, waiting for transfers between devices, outward(): got = lax.all_to_all(tok, PLANE, split_axis=0, concat_axis=0, tiled=True)  46.4 us
    unnamed x20, local copies, waits for them, and re-layouts  21.2 us
    ppermute x3, starting transfers between devices, swapped(): return lax.ppermute(shard, SWAP, pairs)  16.5 us
    all_to_all x2, starting transfers between devices, homeward(): got = lax.all_to_all(got, PLANE, split_axis=0, concat_axis=0, tiled=True)  16.1 us
    convert_element_type x1, other arithmetic, shards(): (value_slope * gelu_slope(value_arg)).astype(jnp.bfloat16)[None]  15.5 us
    all_to_all x2, starting transfers between devices, outward(): got = lax.all_to_all(tok, PLANE, split_axis=0, concat_axis=0, tiled=True)  14.5 us
  transfers between devices with their start and end apart: 9, of which 5 were waited for; matrix products, arithmetic and copies ran while one was open for 25% of the time, Pallas kernels for 0%

profile of v1, /device:TPU:47, one launch (start us, length us, event | category | flops | bytes accessed | tf_op | source)
XLA Modules:
  0.0 385.7 jit_solution(6176144169898661657)
XLA Ops:
  7.2 6.9 %collective-permute-start = (bf16[128,1024]{1,0:T(8,128)(2,1)}, bf16[128,1024]{1,0:T(8,128)(2,1)S(1)}, u32[]{:S(2)}, u32[]{:S(2)}) collective-permute-start(bf16[128,1024]{1,0:T(8,128)(2,1)} %bitcast.165), channel_id=1, source_target_pairs={{0,0},{1,32},{2,64},{3,96},{4,128},{5,160},{6,192},{7,224},{32,1},... | collective-permute-start | bytes 786440 | tf_op jit(solution)/shard_map/ppermute | solution.py:30
  17.5 15.1 %collective-permute-done = bf16[128,1024]{1,0:T(8,128)(2,1)S(1)} collective-permute-done((bf16[128,1024]{1,0:T(8,128)(2,1)}, bf16[128,1024]{1,0:T(8,128)(2,1)S(1)}, u32[]{:S(2)}, u32[]{:S(2)}) %collective-permute-start) | collective-permute-done | bytes 262176 | tf_op jit(solution)/shard_map/ppermute | solution.py:30
  33.3 10.0 %fusion.10 = bf16[256,4096]{0,1:T(8,128)(2,1)} fusion(bf16[1,256,4096]{1,2,0:T(8,128)(2,1)S(1)} %copy.39), kind=kLoop, calls=%fused_computation.29 | loop fusion | flops 69206016 | bytes 4194304 | tf_op jit(solution)/shard_map/convert_element_type | solution.py:46
  43.3 4.1 %copy.33 = bf16[1,256,4096]{1,2,0:T(8,128)(2,1)} copy(bf16[1,256,4096]{2,1,0:T(8,128)(2,1)} %param.6) | data formatting | bytes 4194304 | tf_op args[0]
  47.4 4.1 %fusion.1 = bf16[256,4096]{0,1:T(8,128)(2,1)} fusion(bf16[256,4096]{0,1:T(8,128)(2,1)} %fusion.10, bf16[1,256,4096]{1,2,0:T(8,128)(2,1)} %copy.33), kind=kLoop, calls=%fused_computation.20 | loop fusion | flops 4194304 | bytes 6291456 | tf_op jit(solution)/shard_map/convert_element_type | solution.py:51
  51.5 7.0 %all-to-all-start.2 = ((bf16[32,256,128]{1,2,0:T(8,128)(2,1)}), bf16[32,256,128]{1,2,0:T(8,128)(2,1)}, u32[]{:S(2)}, u32[]{:S(2)}) async-start(bf16[32,256,128]{1,2,0:T(8,128)(2,1)} %bitcast.155), calls=%async_computation.2 | async-start | bytes 4194304 | tf_op jit(solution)/shard_map/all_to_all | solution.py:55
  61.9 22.7 %all-to-all-done.2 = bf16[32,256,128]{1,2,0:T(8,128)(2,1)} async-done(((bf16[32,256,128]{1,2,0:T(8,128)(2,1)}), bf16[32,256,128]{1,2,0:T(8,128)(2,1)}, u32[]{:S(2)}, u32[]{:S(2)}) %all-to-all-start.2) | async-done | bytes 2097184 | tf_op jit(solution)/shard_map/all_to_all | solution.py:55
  88.6 6.0 %convert_bitcast_fusion.1 = bf16[8,1024,128]{1,2,0:T(8,128)(2,1)} fusion(bf16[8,1024,128]{2,1,0:T(8,128)(2,1)} %bitcast.158, bf16[1024,1024]{1,0:T(8,128)(2,1)} %all-gather.2.cloned.1.call-done), kind=kOutput, calls=%fused_computation.165 | convolution fusion | flops 2148532224 | bytes 6291456 | tf_op jit(solution)/shard_map/pq,npc->nqc/dot_general | solution.py:65
  102.5 7.5 %all-to-all-start.3 = ((bf16[32,256,128]{1,2,0:T(8,128)(2,1)}), bf16[32,256,128]{1,2,0:T(8,128)(2,1)}, u32[]{:S(2)}, u32[]{:S(2)}) async-start(bf16[32,256,128]{1,2,0:T(8,128)(2,1)} %copy.43), calls=%async_computation.3 | async-start | bytes 4194304 | tf_op jit(solution)/shard_map/all_to_all | solution.py:60
  110.0 9.4 %fusion.7 = f32[256]{0:T(256)S(1)} fusion(bf16[1,256,4096]{1,2,0:T(8,128)(2,1)S(1)} %copy.34), kind=kLoop, calls=%fused_computation.26 | loop fusion | flops 70254336 | bytes 2098176 | tf_op jit(solution)/shard_map/reduce_sum | solution.py:48
  123.2 12.8 %all-to-all-done.3 = bf16[32,256,128]{1,2,0:T(8,128)(2,1)} async-done(((bf16[32,256,128]{1,2,0:T(8,128)(2,1)}), bf16[32,256,128]{1,2,0:T(8,128)(2,1)}, u32[]{:S(2)}, u32[]{:S(2)}) %all-to-all-start.3) | async-done | bytes 2097184 | tf_op jit(solution)/shard_map/all_to_all | solution.py:60
  136.0 11.6 %fusion.61 = (f32[32,128]{1,0:T(8,128)S(1)}, f32[256]{0:T(256)S(1)}, f32[256,32,128]{0,2,1:T(8,128)S(1)}) fusion(bf16[32,256,128]{1,2,0:T(8,128)(2,1)} %all-to-all-done.3, f32[256]{0:T(256)S(1)} %get-tuple-element.31, f32[32,128]{1,0:T(8,128)S(1)} %bitcast.162, f32[256,32,128]{0,2,1:T(8,128)} %bitcast.154, f32[256,32,128]{0,2,1:T(8,128)} %bitcast.153), kind=kLoop, calls=%fused_computation.83 | loop fusion | flops 71298816 | bytes 14714880 | tf_op jit(solution)/shard_map/reduce_sum | solution.py:84
  149.3 7.5 %all-to-all-start = ((bf16[32,256,128]{1,2,0:T(8,128)(2,1)}), bf16[32,256,128]{1,2,0:T(8,128)(2,1)}, u32[]{:S(2)}, u32[]{:S(2)}) async-start(bf16[32,256,128]{1,2,0:T(8,128)(2,1)} %fusion.121), calls=%async_computation | async-start | bytes 4194304 | tf_op jit(solution)/shard_map/all_to_all | solution.py:55
  159.0 23.7 %all-to-all-done = bf16[32,256,128]{1,2,0:T(8,128)(2,1)} async-done(((bf16[32,256,128]{1,2,0:T(8,128)(2,1)}), bf16[32,256,128]{1,2,0:T(8,128)(2,1)}, u32[]{:S(2)}, u32[]{:S(2)}) %all-to-all-start) | async-done | bytes 2097184 | tf_op jit(solution)/shard_map/all_to_all | solution.py:55
  186.8 4.6 %convolution_bitcast_fusion = f32[1024,1024]{0,1:T(8,128)S(1)} fusion(bf16[8,1024,128]{2,1,0:T(8,128)(2,1)} %bitcast.159, bf16[8,1024,128]{2,1,0:T(8,128)(2,1)} %bitcast.160), kind=kOutput, calls=%fused_computation.158 | convolution fusion | flops 2147483648 | bytes 8388608 | tf_op jit(solution)/shard_map/npc,nqc->pq/dot_general | solution.py:72
  194.6 5.6 %collective-permute-start.1 = (f32[1,1024]{1,0:T(1,128)S(1)}, f32[1,1024]{1,0:T(1,128)S(1)}, u32[]{:S(2)}, u32[]{:S(2)}) collective-permute-start(f32[1,1024]{1,0:T(1,128)S(1)} %copy-done.6), channel_id=1, source_target_pairs={{0,0},{1,32},{2,64},{3,96},{4,128},{5,160},{6,192},{7,224},{32,1},... | collective-permute-start | bytes 12296 | tf_op jit(solution)/shard_map/ppermute | solution.py:30
  200.2 4.1 %convert_element_type.124 = f32[32,256,128]{1,2,0:T(8,128)} convert(bf16[32,256,128]{1,2,0:T(8,128)(2,1)} %all-to-all-done.3) | non-fusion elementwise | flops 1048576 | bytes 6291456 | tf_op jit(solution)/shard_map/convert_element_type | solution.py:68
  212.0 8.6 %all-to-all-start.1 = ((bf16[32,256,128]{2,1,0:T(8,128)(2,1)}), bf16[32,256,128]{2,1,0:T(8,128)(2,1)}, u32[]{:S(2)}, u32[]{:S(2)}) async-start(bf16[32,256,128]{2,1,0:T(8,128)(2,1)} %bitcast.156), calls=%async_computation.1 | async-start | bytes 4194304 | tf_op jit(solution)/shard_map/all_to_all | solution.py:60
  220.6 15.5 %fusion.17 = bf16[1,256,4096]{1,2,0:T(8,128)(2,1)} fusion(bf16[1,256,4096]{1,2,0:T(8,128)(2,1)S(1)} %copy.34, f32[256]{0:T(256)S(1)} %broadcast_multiply_fusion, f32[256]{0:T(256)S(1)} %get-tuple-element.30, f32[4096]{0:T(1024)S(1)} %copy-done.4, f32[256]{0:T(256)S(1)} %get-tuple-element.31, f32[1,256,4096]{1,2,0:T(8,128)} %bitcast.152), kind=kLoop, calls=%fused_computation.36 | loop fusion | flops 83886080 | bytes 8408064 | tf_op jit(solution)/shard_map/convert_element_type | solution.py:89
  240.2 76.8 %psum.7 = f32[4096]{0:T(1024)} all-reduce(f32[4096]{0:T(1024)S(1)} %bitcast.164), channel_id=1, replica_groups=mesh['sp_0'=8,'sp_1'=4,'dp_0'=4,'dp_1'=2] {'sp_0','sp_1','dp_0','dp_1'}, use_global_device_ids=true, to_apply=%region_6.7 | all-reduce | flops 4096 | bytes 32768 | tf_op jit(solution)/shard_map/psum | solution.py:84
  321.1 5.7 %copy.38 = f32[256,32,128]{0,2,1:T(8,128)} copy(f32[256,32,128]{2,0,1:T(8,128)} %convert_bitcast_fusion) | data formatting | bytes 8388608 | tf_op jit(solution)/shard_map/convert_element_type | solution.py:71
  326.8 4.8 %fusion = bf16[256,4096]{0,1:T(8,128)(2,1)} fusion(f32[256,32,128]{0,2,1:T(8,128)} %copy.38, bf16[1,256,4096]{1,2,0:T(8,128)(2,1)} %copy.33), kind=kLoop, calls=%fused_computation.19 | loop fusion | flops 3145728 | bytes 8388608 | tf_op jit(solution)/shard_map/convert_element_type | solution.py:82
  335.5 4.2 %fusion.127 = bf16[1,256,4096]{1,2,0:T(8,128)(2,1)} fusion(bf16[1,256,4096]{1,2,0:T(8,128)(2,1)S(1)} %copy-done.1, bf16[256,4096]{0,1:T(8,128)(2,1)} %fusion), kind=kLoop, calls=%fused_computation.166 | loop fusion | flops 12582912 | bytes 6291456 | tf_op jit(solution)/shard_map/broadcast_in_dim | solution.py:83
  343.8 33.5 %collective-permute-done.2 = f32[128,1152]{0,1:T(8,128)S(1)} collective-permute-done((f32[128,1152]{0,1:T(8,128)}, f32[128,1152]{0,1:T(8,128)S(1)}, u32[]{:S(2)}, u32[]{:S(2)}) %collective-permute-start.2) | collective-permute-done | bytes 589856 | tf_op jit(solution)/shard_map/ppermute | solution.py:30
  (46 shorter events, 59.7 us)
Async XLA Ops:
  7.2 81.4 %all-gather.2.cloned.1.call-start = ((), (), s32[]{:S(2)}) async-start(), calls=%async_computation.5 | async-start | bytes 2359296 | tf_op jit(solution)/shard_map/all_gather | solution.py:40
  7.2 25.4 %collective-permute-start = (bf16[128,1024]{1,0:T(8,128)(2,1)}, bf16[128,1024]{1,0:T(8,128)(2,1)S(1)}, u32[]{:S(2)}, u32[]{:S(2)}) collective-permute-start(bf16[128,1024]{1,0:T(8,128)(2,1)} %bitcast.165), channel_id=1, source_target_pairs={{0,0},{1,32},{2,64},{3,96},{4,128},{5,160},{6,192},{7,224},{32,1},... | collective-permute-start | bytes 786440 | tf_op jit(solution)/shard_map/ppermute | solution.py:30
  17.4 30.0 %copy-start = (bf16[1,256,4096]{1,2,0:T(8,128)(2,1)}, bf16[1,256,4096]{1,2,0:T(8,128)(2,1)S(1)}, u32[]{:S(2)}) copy-start(bf16[1,256,4096]{1,2,0:T(8,128)(2,1)S(1)} %copy.39) | copy-start | bytes 6291460
  32.6 0.7 copy-start.3
  51.5 33.0 %all-to-all-start.2 = ((bf16[32,256,128]{1,2,0:T(8,128)(2,1)}), bf16[32,256,128]{1,2,0:T(8,128)(2,1)}, u32[]{:S(2)}, u32[]{:S(2)}) async-start(bf16[32,256,128]{1,2,0:T(8,128)(2,1)} %bitcast.155), calls=%async_computation.2 | async-start | bytes 4194304 | tf_op jit(solution)/shard_map/all_to_all | solution.py:55
  102.5 33.5 %all-to-all-start.3 = ((bf16[32,256,128]{1,2,0:T(8,128)(2,1)}), bf16[32,256,128]{1,2,0:T(8,128)(2,1)}, u32[]{:S(2)}, u32[]{:S(2)}) async-start(bf16[32,256,128]{1,2,0:T(8,128)(2,1)} %copy.43), calls=%async_computation.3 | async-start | bytes 4194304 | tf_op jit(solution)/shard_map/all_to_all | solution.py:60
  119.4 16.6 %copy-start.4 = (f32[4096]{0:T(1024)S(1)}, f32[4096]{0:T(1024)}, u32[]{:S(2)}) copy-start(f32[4096]{0:T(1024)} %param.11) | copy-start | bytes 49156
  149.3 33.5 %all-to-all-start = ((bf16[32,256,128]{1,2,0:T(8,128)(2,1)}), bf16[32,256,128]{1,2,0:T(8,128)(2,1)}, u32[]{:S(2)}, u32[]{:S(2)}) async-start(bf16[32,256,128]{1,2,0:T(8,128)(2,1)} %fusion.121), calls=%async_computation | async-start | bytes 4194304 | tf_op jit(solution)/shard_map/all_to_all | solution.py:55
  156.8 174.8 %reduce-scatter.2.cloned.1.call-start = ((), (), s32[]{:S(2)}) async-start(), calls=%async_computation.6 | async-start | bytes 5308416 | tf_op jit(solution)/shard_map/reduce_scatter | solution.py:77
  193.9 0.7 copy-start.6
  194.6 9.8 %copy-start.2 = (bf16[32,256,128]{2,1,0:T(8,128)(2,1)S(1)}, bf16[32,256,128]{2,1,0:T(8,128)(2,1)}, u32[]{:S(2)}) copy-start(bf16[32,256,128]{2,1,0:T(8,128)(2,1)} %copy.35) | copy-start | bytes 6291460
  194.6 9.8 %copy-start.5 = (bf16[1024,1024]{1,0:T(8,128)(2,1)S(1)}, bf16[1024,1024]{1,0:T(8,128)(2,1)}, u32[]{:S(2)}) copy-start(bf16[1024,1024]{1,0:T(8,128)(2,1)} %all-gather.2.cloned.1.call-done) | copy-start | bytes 6291460
  194.6 9.8 %collective-permute-start.1 = (f32[1,1024]{1,0:T(1,128)S(1)}, f32[1,1024]{1,0:T(1,128)S(1)}, u32[]{:S(2)}, u32[]{:S(2)}) collective-permute-start(f32[1,1024]{1,0:T(1,128)S(1)} %copy-done.6), channel_id=1, source_target_pairs={{0,0},{1,32},{2,64},{3,96},{4,128},{5,160},{6,192},{7,224},{32,1},... | collective-permute-start | bytes 12296 | tf_op jit(solution)/shard_map/ppermute | solution.py:30
  212.0 105.0 %all-to-all-start.1 = ((bf16[32,256,128]{2,1,0:T(8,128)(2,1)}), bf16[32,256,128]{2,1,0:T(8,128)(2,1)}, u32[]{:S(2)}, u32[]{:S(2)}) async-start(bf16[32,256,128]{2,1,0:T(8,128)(2,1)} %bitcast.156), calls=%async_computation.1 | async-start | bytes 4194304 | tf_op jit(solution)/shard_map/all_to_all | solution.py:60
  326.8 8.7 %copy-start.1 = (bf16[1,256,4096]{1,2,0:T(8,128)(2,1)S(1)}, bf16[1,256,4096]{1,2,0:T(8,128)(2,1)}, u32[]{:S(2)}) copy-start(bf16[1,256,4096]{1,2,0:T(8,128)(2,1)} %copy-done) | copy-start | bytes 6291460
  331.6 45.7 %collective-permute-start.2 = (f32[128,1152]{0,1:T(8,128)}, f32[128,1152]{0,1:T(8,128)S(1)}, u32[]{:S(2)}, u32[]{:S(2)}) collective-permute-start(f32[128,1152]{0,1:T(8,128)} %reduce-scatter.2.cloned.1.call-done), channel_id=1, source_target_pairs={{0,0},{1,32},{2,64},{3,96},{4,128},{5,160},{6,192},{7,224},{32,1},... | collective-permute-start | bytes 1769480 | tf_op jit(solution)/shard_map/ppermute | solution.py:30
Sparse Core Ops, SparseCore 0:
  33.4 36.1 all-gather.1
  194.1 58.9 reduce-scatter.1

commit v2 on v1

v2 whole, which is shorter than its diff:
```python
import math

import jax
import jax.numpy as jnp
from jax import lax
from jax.experimental import pallas as pl
from jax.experimental.pallas import tpu as pltpu
from jax.sharding import Mesh
from jax.sharding import PartitionSpec as P

SP = ("sp_0", "sp_1")
DP = ("dp_0", "dp_1")

NZ, NY, NX, NC = 8, 4, 4, 2
NI = NX * NC
ROWS = 256
DIM = 128
WIDTH = NI * NY * DIM
CHUNK = NY * DIM
BLOCK = NY * ROWS
PART = BLOCK // NZ
F32, BF16 = jnp.float32, jnp.bfloat16

norm_floor = 0.5
root_half = 1.0 / math.sqrt(2.0)
inv_root_tau = 1.0 / math.sqrt(2.0 * math.pi)

ORDER = ((0, 0), (0, 1), (1, 0), (3, 0), (1, 1), (3, 1), (2, 0), (2, 1))
NT = (((1,), (1,)), ((), ()))


def phi(x):
    return 0.5 * (1.0 + lax.erf(x * root_half))


def slope(x):
    return phi(x) + x * jnp.exp(-0.5 * x * x) * inv_root_tau


def kernel(
    cot_hbm, up_hbm, val_hbm, w_hbm, bias_hbm, gain_hbm,
    upg_hbm, valg_hbm, wg_hbm, bg_hbm, gg_hbm,
    cot, up, val, w_own, b_own, gain,
    S, X, Y, R, H, B,
    w_in, b_in, W, WT, bcol,
    wga, ws, wr, wsum, wout, bsend, br, bsum, bout,
    gsend, gz, gxs, gx, gys, gy,
    act, su, sv, inv, dot, gacc,
    in_sem, out_sem,
    xo_send, xo_recv, yo_send, yo_recv,
    sw_send, sw_recv, wz_send, wz_recv,
    yr_send, yr_recv, xr_send, xr_recv,
    gr_send, gr_recv, so_send, so_recv,
    gn_send, gn_recv,
):
    z, y, x, c = (lax.axis_index(a) for a in ("sp_0", "sp_1", "dp_0", "dp_1"))
    me = x * NC + c

    def remote(src, dst, send, recv, where):
        return pltpu.make_async_remote_copy(
            src_ref=src, dst_ref=dst, send_sem=send, recv_sem=recv,
            device_id=where, device_id_type=pl.DeviceIdType.MESH,
        )

    def at_xc(dx, dc):
        return lax.rem(x + dx, NX), lax.rem(c + dc, NC)

    def from_xc(dx, dc):
        return lax.rem(x + NX - dx, NX), lax.rem(c + NC - dc, NC)

    def wait(ref, sem):
        pltpu.make_async_copy(ref, ref, sem).wait()

    loads = [
        pltpu.make_async_copy(src, dst, in_sem.at[k])
        for k, (src, dst) in enumerate(
            ((up_hbm, up), (cot_hbm, cot), (w_hbm, w_own), (bias_hbm, b_own), (val_hbm, val), (gain_hbm, gain))
        )
    ]
    for load in loads:
        load.start()

    barrier = pltpu.get_barrier_semaphore()

    def greet(where):
        pl.semaphore_signal(barrier, inc=1, device_id=where, device_id_type=pl.DeviceIdType.MESH)

    for dx, dc in ORDER[1:]:
        xi, ci = at_xc(dx, dc)
        greet({"dp_0": xi, "dp_1": ci})
    for dy in range(1, NY):
        greet({"sp_1": lax.rem(y + dy, NY)})
    for dz in range(1, NZ):
        greet({"sp_0": lax.rem(z + dz, NZ)})
    swap_to = {"sp_0": me, "dp_0": z // NC, "dp_1": lax.rem(z, NC)}

    @pl.when(me != z)
    def _():
        greet(swap_to)

    peers = NI - 1 + NY - 1 + NZ - 1

    @pl.when(me != z)
    def _():
        pl.semaphore_wait(barrier, peers + 1)

    @pl.when(me == z)
    def _():
        pl.semaphore_wait(barrier, peers)

    loads[2].wait()
    loads[3].wait()
    moves = ((w_own, w_in), (b_own, b_in))

    @pl.when(me != z)
    def _():
        for k, (src, dst) in enumerate(moves):
            remote(src, dst, sw_send.at[k], sw_recv.at[k], swap_to).start()

    @pl.when(me == z)
    def _():
        for k, (src, dst) in enumerate(moves):
            pltpu.make_async_copy(src, dst, sw_recv.at[k]).start()

    def cols(i):
        return pl.ds(pl.multiple_of(i * CHUNK, CHUNK), CHUNK)

    def gate_chunk(i):
        @pl.loop(0, ROWS // 32)
        def _(t):
            rows = pl.ds(pl.multiple_of(t * 32, 32), 32)
            u = up[rows, cols(i)].astype(F32)
            u = (u * phi(u)).astype(BF16).astype(F32)
            g = (cot[rows, cols(i)].astype(F32) * u).astype(BF16)
            for k in range(NY):
                S[0, i, k, rows, :] = g[:, k * DIM : (k + 1) * DIM]

    def slot(xs, cs, row):
        return (
            xs,
            pl.ds(pl.multiple_of(row * ROWS, ROWS), ROWS),
            pl.ds(pl.multiple_of(cs * DIM, DIM), DIM),
        )

    def forward(a, buf, n, d):
        xs, cs = from_xc(*d)
        s = xs * NC + cs
        for dy in range(1, NY):
            to = lax.rem(y + dy, NY)
            remote(
                buf.at[a, s, to], Y.at[(a, *slot(xs, cs, y))],
                yo_send, yo_recv.at[a, d[0]], {"sp_1": to},
            ).start()
        pltpu.make_async_copy(buf.at[a, s, y], Y.at[(a, *slot(xs, cs, y))], yo_recv.at[a, d[0]]).start()

    def push(a, n):
        d = ORDER[n]
        if n == 0:
            forward(a, S, n, d)
            return
        xi, ci = at_xc(*d)
        remote(
            S.at[a, xi * NC + ci], X.at[a, me], xo_send, xo_recv.at[a, n], {"dp_0": xi, "dp_1": ci}
        ).start()

    def relay(a, n):
        xs, cs = from_xc(*ORDER[n])
        wait(X.at[a, xs * NC + cs], xo_recv.at[a, n])
        forward(a, X, n, ORDER[n])

    loads[0].wait()
    loads[1].wait()
    for n, d in enumerate(ORDER):
        xi, ci = at_xc(*d)
        gate_chunk(xi * NC + ci)
        if n > 0:
            push(0, n - 1)
    loads[4].wait()
    loads[5].wait()

    wait(w_in, sw_recv.at[0])
    wait(b_in, sw_recv.at[1])
    push(0, NI - 1)
    for dz in range(1, NZ):
        remote(w_in, W.at[z], wz_send, wz_recv, {"sp_0": lax.rem(z + dz, NZ)}).start()
    pltpu.make_async_copy(w_in, W.at[z], wz_recv).start()

    @pl.loop(0, ROWS // 16)
    def _(t):
        rows = pl.ds(pl.multiple_of(t * 16, 16), 16)
        total = jnp.zeros((16, DIM), F32)
        for i in range(NI):
            v = val[rows, i * CHUNK : (i + 1) * CHUNK].astype(F32)
            v = v * phi(v)
            act[rows, i * CHUNK : (i + 1) * CHUNK] = v
            v = v * v
            for k in range(NY):
                total += v[:, k * DIM : (k + 1) * DIM]
        scale = lax.rsqrt(jnp.sum(total, axis=1, keepdims=True) / WIDTH + norm_floor)
        inv[rows, :] = jnp.broadcast_to(scale, (16, DIM))
        for i in range(NI):
            for k in range(NY):
                at = slice((i * NY + k) * DIM, (i * NY + k + 1) * DIM)
                S[1, i, k, rows, :] = (act[rows, at] * scale * gain[0:1, at]).astype(BF16)

    for n in range(2, NI):
        push(1, n)
    push(1, 1)
    push(1, 0)

    def slopes(src, dst):
        @pl.loop(0, ROWS // 32 * NI)
        def _(t):
            rows = pl.ds(pl.multiple_of(t // NI * 32, 32), 32)
            at = cols(lax.rem(t, NI))
            dst[rows, at] = slope(src[rows, at].astype(F32))

    for n in range(1, 6):
        relay(0, n)
    slopes(up, su)
    relay(1, 1)
    for n in (6, 7):
        relay(0, n)
    slopes(val, sv)
    for n in range(2, 6):
        relay(1, n)

    for k in range(BLOCK // DIM):
        part = jnp.broadcast_to(b_in[0:1, k * DIM : (k + 1) * DIM], (DIM, DIM))
        bcol[k * DIM : (k + 1) * DIM, :] = jnp.transpose(part)

    def pair(dx):
        return lax.rem(x + NX - dx, NX)

    for dx in (0, 1, 3):
        for a in range(2):
            wait(Y.at[a, pair(dx)], yo_recv.at[a, dx])

    def tile(t):
        return pl.ds(pl.multiple_of(t * ROWS, ROWS), ROWS)

    def outer(p, i, j):
        return lax.dot_general(Y[0, p, tile(i), :], Y[1, p, tile(j), :], NT, preferred_element_type=F32)

    @pl.loop(0, NY * NY)
    def _(t):
        i, j = t // NY, lax.rem(t, NY)
        wga[tile(i), tile(j)] = outer(pair(0), i, j) + outer(pair(1), i, j) + outer(pair(3), i, j)

    ones = jnp.ones((8, NC * DIM), BF16)

    def row_sums(dx):
        return lax.dot_general(ones, Y[0, pair(dx)], NT, preferred_element_type=F32)

    bsum[...] = row_sums(0) + row_sums(1) + row_sums(3)

    for n in (6, 7):
        relay(1, n)
    wait(W, wz_recv)

    @pl.loop(0, NZ)
    def _(j):
        WT[:, pl.ds(pl.multiple_of(j * PART, PART), PART)] = jnp.transpose(W[j])

    for a in range(2):
        wait(Y.at[a, pair(2)], yo_recv.at[a, 2])

    @pl.loop(0, NY * NY)
    def _(t):
        i, j = t // NY, lax.rem(t, NY)
        total = (wga[tile(i), tile(j)] + outer(pair(2), i, j)).astype(BF16)
        ws[i * 2, :, tile(j)] = total[:PART]
        ws[i * 2 + 1, :, tile(j)] = total[PART:]

    bsum[...] += row_sums(2)
    for j in range(NZ):
        bsend[j] = bsum[:, j * DIM : (j + 1) * DIM]
    for dz in range(1, NZ):
        to = lax.rem(z + dz, NZ)
        remote(ws.at[to], wr.at[z], gr_send.at[0], gr_recv.at[0], {"sp_0": to}).start()
        remote(bsend.at[to], br.at[z], gr_send.at[1], gr_recv.at[1], {"sp_0": to}).start()
    pltpu.make_async_copy(ws.at[z], wr.at[z], gr_recv.at[0]).start()
    pltpu.make_async_copy(bsend.at[z], br.at[z], gr_recv.at[1]).start()

    gacc[...] = jnp.zeros_like(gacc)
    for a in range(2):
        for dx in (2, 1, 3, 0):
            xs = pair(dx)

            @pl.loop(0, NY)
            def _(t):
                if a == 0:
                    part = jnp.dot(WT[tile(t), :], Y[0, xs], preferred_element_type=F32).astype(BF16)
                    prod = part.astype(F32) * Y[1, xs, tile(t), :].astype(F32)
                    gacc[...] += jnp.sum(prod.reshape(ROWS // 8, 8, NC * DIM), axis=0)
                else:
                    rows = jnp.concatenate([W[t * 2], W[t * 2 + 1]], axis=0)
                    part = jnp.dot(rows, Y[1, xs], preferred_element_type=F32)
                    col = bcol[tile(t), :]
                    part = (part + jnp.concatenate([col, col], axis=1)).astype(BF16)
                R[a, xs, t, 0] = part[:, :DIM]
                R[a, xs, t, 1] = part[:, DIM:]

            for dy in range(1, NY):
                to = lax.rem(y + dy, NY)
                remote(R.at[a, xs, to], H.at[a, xs, y], yr_send, yr_recv.at[a, dx], {"sp_1": to}).start()
            pltpu.make_async_copy(R.at[a, xs, y], H.at[a, xs, y], yr_recv.at[a, dx]).start()
        if a == 0:
            line = jnp.sum(gacc[...], axis=0, keepdims=True)
            mine = pl.ds(pl.multiple_of((me * NY + y) * DIM, DIM), DIM)
            line = (line[:, :DIM] + line[:, DIM:]) / gain[0:1, mine]
            gsend[...] = jnp.broadcast_to(line, (8, DIM))
            for dz in range(1, NZ):
                remote(gsend, gz.at[z], gn_send.at[0], gn_recv.at[0], {"sp_0": lax.rem(z + dz, NZ)}).start()
            pltpu.make_async_copy(gsend, gz.at[z], gn_recv.at[0]).start()

    def home(a, dx):
        wait(H.at[a, pair(dx)], yr_recv.at[a, dx])
        xs = pair(dx)
        back_dx = (NX - dx) % NX
        for dc in range(NC):
            n = ORDER.index((back_dx, dc))
            cs = lax.rem(c + dc, NC)
            if n == 0:
                pltpu.make_async_copy(H.at[a, xs, :, cs], B.at[a, me], xr_recv.at[a, n]).start()
            else:
                remote(
                    H.at[a, xs, :, cs], B.at[a, me], xr_send, xr_recv.at[a, n],
                    {"dp_0": xs, "dp_1": cs},
                ).start()

    def arrived(a, n):
        xs, cs = from_xc(*ORDER[n])
        s = xs * NC + cs
        wait(B.at[a, s], xr_recv.at[a, n])
        return s

    for dx in (2, 1, 3, 0):
        home(0, dx)

    wait(gz, gn_recv.at[0])
    gxs[...] = jnp.sum(gz[...], axis=0)
    for n, d in enumerate(ORDER):
        xi, ci = at_xc(*d)
        if n == 0:
            pltpu.make_async_copy(gxs, gx.at[me], gn_recv.at[1]).start()
        else:
            remote(gxs, gx.at[me], gn_send.at[1], gn_recv.at[1], {"dp_0": xi, "dp_1": ci}).start()

    dot[...] = jnp.zeros_like(dot)
    for n in (0, 1, 2, 3, 4, 5, 6, 7):
        s = arrived(0, n)

        @pl.loop(0, ROWS // 32)
        def _(t):
            rows = pl.ds(pl.multiple_of(t * 32, 32), 32)
            total = dot[rows, :]
            for k in range(NY):
                at = pl.ds(pl.multiple_of((s * NY + k) * DIM, DIM), DIM)
                total += B[0, s, k, rows, :].astype(F32) * gain[0:1, at] * act[rows, at]
            dot[rows, :] = total

        if n == 3:
            home(1, 2)

    for dx in (1, 3, 0):
        home(1, dx)

    wait(gx, gn_recv.at[1])
    for i in range(NI):
        gys[i : i + 1, :] = gx[i, 0:1, :]
    for dy in range(1, NY):
        remote(gys, gy.at[y], gn_send.at[2], gn_recv.at[2], {"sp_1": lax.rem(y + dy, NY)}).start()
    pltpu.make_async_copy(gys, gy.at[y], gn_recv.at[2]).start()

    @pl.loop(0, ROWS // 16)
    def _(t):
        rows = pl.ds(pl.multiple_of(t * 16, 16), 16)
        scale = inv[rows, :]
        mean = jnp.sum(dot[rows, :], axis=1, keepdims=True) / WIDTH
        cube = scale * scale * scale * mean
        for g in range(NI * NY):
            at = slice(g * DIM, (g + 1) * DIM)
            scaled = B[0, g // NY, g % NY, rows, :].astype(F32) * gain[0:1, at]
            grad = (scale * scaled - cube * act[rows, at]) * sv[rows, at]
            val[rows, at] = grad.astype(BF16)

    pltpu.make_async_copy(val, valg_hbm, out_sem.at[0]).start()

    for n in (0, 1, 2, 3, 4, 5, 6, 7):
        s = arrived(1, n)

        @pl.loop(0, ROWS // 32)
        def _(t):
            rows = pl.ds(pl.multiple_of(t * 32, 32), 32)
            for k in range(NY):
                at = pl.ds(pl.multiple_of((s * NY + k) * DIM, DIM), DIM)
                mid = (cot[rows, at].astype(F32) * B[1, s, k, rows, :].astype(F32)).astype(BF16)
                up[rows, at] = (mid.astype(F32) * su[rows, at]).astype(BF16)

        pltpu.make_async_copy(up.at[:, cols(s)], upg_hbm.at[:, cols(s)], out_sem.at[1]).start()

    wait(wr, gr_recv.at[0])
    wait(br, gr_recv.at[1])

    @pl.loop(0, PART // 16)
    def _(t):
        rows = pl.ds(pl.multiple_of(t * 16, 16), 16)
        total = wr[0, rows, :].astype(F32)
        for k in range(1, NZ):
            total += wr[k, rows, :].astype(F32)
        wsum[rows, :] = total

    bsum[:, :DIM] = jnp.sum(br[...], axis=0)
    results = ((wsum, wout), (bsum.at[:, pl.ds(0, DIM)], bout))

    @pl.when(me != z)
    def _():
        for k, (src, dst) in enumerate(results):
            remote(src, dst, so_send.at[k], so_recv.at[k], swap_to).start()

    @pl.when(me == z)
    def _():
        for k, (src, dst) in enumerate(results):
            pltpu.make_async_copy(src, dst, so_recv.at[k]).start()

    wait(gy, gn_recv.at[2])
    tail = [pltpu.make_async_copy(gy, gg_hbm, out_sem.at[2])]
    tail[0].start()
    wait(wout, so_recv.at[0])
    wait(bout, so_recv.at[1])
    tail += [
        pltpu.make_async_copy(wout, wg_hbm, out_sem.at[3]),
        pltpu.make_async_copy(bout, bg_hbm, out_sem.at[4]),
    ]
    for copy in tail[1:]:
        copy.start()

    for a in range(2):
        wait(S.at[a, pl.ds(0, NI - 1)], xo_send)
        wait(H.at[a, pl.ds(0, 3)], xr_send)
        wait(H.at[a, 0, pl.ds(0, 2)], xr_send)
        wait(R.at[a, :, pl.ds(0, NY - 1)], yr_send)
        wait(X.at[a, :, pl.ds(0, NY - 1)], yo_send)
    wait(W.at[pl.ds(0, NZ - 1)], wz_send)
    wait(ws.at[pl.ds(0, NZ - 1)], gr_send.at[0])
    wait(bsend.at[pl.ds(0, NZ - 1)], gr_send.at[1])
    wait(gz.at[pl.ds(0, NZ - 1)], gn_send.at[0])
    wait(gx.at[pl.ds(0, NI - 1)], gn_send.at[1])
    wait(gy.at[pl.ds(0, NY - 1)], gn_send.at[2])

    @pl.when(me != z)
    def _():
        for k, (src, dst) in enumerate(moves):
            wait(src, sw_send.at[k])
        for k, (src, dst) in enumerate(results):
            wait(src, so_send.at[k])

    wait(val, out_sem.at[0])
    wait(up, out_sem.at[1])
    for copy in tail:
        copy.wait()


def shards(cotangent, up_pre, value_pre, spatial_weight, spatial_bias, value_gain):
    vmem, dma = pltpu.VMEM, pltpu.SemaphoreType.DMA
    tok = (ROWS, WIDTH)
    out = pl.pallas_call(
        kernel,
        name="gating_backward",
        out_shape=(
            jax.ShapeDtypeStruct(tok, BF16),
            jax.ShapeDtypeStruct(tok, BF16),
            jax.ShapeDtypeStruct((PART, BLOCK), F32),
            jax.ShapeDtypeStruct((8, DIM), F32),
            jax.ShapeDtypeStruct((NY, NI, DIM), F32),
        ),
        in_specs=[pl.BlockSpec(memory_space=pl.ANY)] * 6,
        out_specs=[pl.BlockSpec(memory_space=pl.ANY)] * 5,
        scratch_shapes=[
            vmem(tok, BF16), vmem(tok, BF16), vmem(tok, BF16),
            vmem((PART, BLOCK), BF16), vmem((1, BLOCK), F32), vmem((1, WIDTH), F32),
            vmem((2, NI, NY, ROWS, DIM), BF16),
            vmem((2, NI, NY, ROWS, DIM), BF16),
            vmem((2, NX, BLOCK, NC * DIM), BF16),
            vmem((2, NX, NY, NC, ROWS, DIM), BF16),
            vmem((2, NX, NY, NC, ROWS, DIM), BF16),
            vmem((2, NI, NY, ROWS, DIM), BF16),
            vmem((PART, BLOCK), BF16), vmem((1, BLOCK), F32),
            vmem((NZ, PART, BLOCK), BF16), vmem((BLOCK, BLOCK), BF16), vmem((BLOCK, DIM), F32),
            vmem((BLOCK, BLOCK), F32), vmem((NZ, PART, BLOCK), BF16), vmem((NZ, PART, BLOCK), BF16),
            vmem((PART, BLOCK), F32), vmem((PART, BLOCK), F32),
            vmem((NZ, 8, DIM), F32), vmem((NZ, 8, DIM), F32), vmem((8, BLOCK), F32), vmem((8, DIM), F32),
            vmem((8, DIM), F32), vmem((NZ, 8, DIM), F32), vmem((8, DIM), F32), vmem((NI, 8, DIM), F32),
            vmem((NI, DIM), F32), vmem((NY, NI, DIM), F32),
            vmem(tok, F32), vmem(tok, F32), vmem(tok, F32),
            vmem((ROWS, DIM), F32), vmem((ROWS, DIM), F32), vmem((8, NC * DIM), F32),
            dma((6,)), dma((5,)),
            dma(()), dma((2, NI)), dma(()), dma((2, NX)),
            dma((2,)), dma((2,)), dma(()), dma(()),
            dma(()), dma((2, NX)), dma(()), dma((2, NI)),
            dma((2,)), dma((2,)), dma((2,)), dma((2,)),
            dma((3,)), dma((3,)),
        ],
        compiler_params=pltpu.CompilerParams(
            collective_id=0, has_side_effects=True, vmem_limit_bytes=67043328
        ),
    )(
        cotangent[0], up_pre[0], value_pre[0], spatial_weight[0], spatial_bias, value_gain[None]
    )
    up_grad, value_grad, weight_grad, bias_grad, gain_grad = out
    gain_grad = gain_grad.transpose(1, 0, 2).reshape(WIDTH)
    return up_grad[None], value_grad[None], weight_grad[None], bias_grad[:1], gain_grad


def solution(mesh):
    torus = Mesh(mesh.devices.reshape(NZ, NY, NX, NC), ("sp_0", "sp_1", "dp_0", "dp_1"))
    in_specs = (
        P(DP, SP, None),
        P(DP, SP, None),
        P(DP, SP, None),
        P(SP, DP, None),
        P(SP, None),
        P(),
    )
    out_specs = (P(DP, SP, None), P(DP, SP, None), P(SP, DP, None), P(SP, DP), P())
    return jax.shard_map(
        shards, mesh=torus, in_specs=in_specs, out_specs=out_specs, check_vma=False
    )
```

time: 387 us -> 208 us (0.54)
  the two profiles are of different devices: /device:TPU:47 before, /device:TPU:89 now
where the time goes in v2:
time: 208 us
  Pallas kernels  199 us (96%)
  local copies, waits for them, and re-layouts  7.98 us (4%)
    pallas_call x1, Pallas kernels, shards(): pl.pallas_call(kernel, name='gating_backward', out_shape=(jax.ShapeDtypeS...  199 us
    unnamed x7, local copies, waits for them, and re-layouts  5.47 us

profile of v2, /device:TPU:89, one launch (start us, length us, event | category | flops | bytes accessed | tf_op | source)
XLA Modules:
  0.0 207.9 jit_solution(10742421890244858429)
XLA Ops:
  0.6 199.3 %gating_backward.1 = (bf16[256,4096]{1,0:T(8,128)(2,1)}, bf16[256,4096]{1,0:T(8,128)(2,1)}, f32[128,1024]{1,0:T(8,128)}, f32[8,128]{1,0:T(8,128)}, f32[4,8,128]{2,1,0:T(8,128)}) custom-call(bf16[256,4096]{1,0:T(8,128)(2,1)} %bitcast.12, bf16[256,4096]{1,0:T(8,128)(2,1)} %bitcast.13, bf16[256,4096]{1,0:T(8,128)(2,1)} %bitcast.14, bf16[128,1024]{1,0:T(8,128)(2,1)} %bitcast.16, ...), custom_call_target="tpu_custom_call" | custom-call | tf_op jit(solution)/shard_map/gating_backward/pallas_call | solution.py:468
  199.9 1.2 slice.3
  201.1 1.3 copy.11
  202.4 0.0 copy-start
  202.4 3.3 %copy.15 = bf16[1,256,4096]{2,1,0:T(8,128)(2,1)} copy(bf16[1,256,4096]{2,1,0:T(8,128)(2,1)} %bitcast.11) | data formatting | bytes 4194304
  205.7 0.0 copy-done
  205.7 0.0 copy-start.1
  205.7 1.3 copy.16
  207.0 0.1 copy-done.1
  207.1 0.8 copy.17
Async XLA Ops:
  202.4 3.3 %copy-start = (bf16[256,4096]{1,0:T(8,128)(2,1)S(1)}, bf16[256,4096]{1,0:T(8,128)(2,1)}, u32[]{:S(2)}) copy-start(bf16[256,4096]{1,0:T(8,128)(2,1)} %get-tuple-element.11) | copy-start | bytes 6291460
  205.7 1.4 copy-start.1

commit v3 on v2

v3 whole, which is shorter than its diff:
```python
import math

import jax
import jax.numpy as jnp
from jax import lax
from jax.experimental import pallas as pl
from jax.experimental.pallas import tpu as pltpu
from jax.sharding import Mesh
from jax.sharding import PartitionSpec as P

SP = ("sp_0", "sp_1")
DP = ("dp_0", "dp_1")

NZ, NY, NX, NC = 8, 4, 4, 2
NI = NX * NC
ROWS = 256
DIM = 128
WIDTH = NI * NY * DIM
CHUNK = NY * DIM
BLOCK = NY * ROWS
PART = BLOCK // NZ
F32, BF16 = jnp.float32, jnp.bfloat16

norm_floor = 0.5
root_half = 1.0 / math.sqrt(2.0)
inv_root_tau = 1.0 / math.sqrt(2.0 * math.pi)

ORDER = ((0, 0), (0, 1), (1, 0), (3, 0), (1, 1), (3, 1), (2, 0), (2, 1))
NT = (((1,), (1,)), ((), ()))


def phi(x):
    return 0.5 * (1.0 + lax.erf(x * root_half))


def slope(x):
    return phi(x) + x * jnp.exp(-0.5 * x * x) * inv_root_tau


def kernel(
    cot_hbm, up_hbm, val_hbm, w_hbm, bias_hbm, gain_hbm,
    upg_hbm, valg_hbm, wg_hbm, bg_hbm, gg_hbm,
    cot, up, val, w_own, b_own, gain,
    S, X, V, Y, R0, R1, H0, H1, B,
    w_in, b_in, W, WT, bcol,
    ws, wr, far3, far4, wsum, wmid, wout, wfin, bsend, br, bsum, bmid, bout,
    gsend, gz, gxs, gx, gys, gy, gall,
    act, su, sv, inv, dot, gacc,
    in_sem, out_sem,
    xo_send, xo_recv, yo_send, yo_recv, vy_send, vy_recv, vx_send, vx_recv,
    sw_send, sw_recv, wz_send, wz_recv,
    yr_send, yr_recv, xr_send, xr_recv, mx_send, mx_recv, my_send, my_recv,
    gr_send, gr_recv, bi_send, bi_recv, so_send, so_recv,
    gn_send, gn_recv,
):
    z, y, x, c = (lax.axis_index(a) for a in ("sp_0", "sp_1", "dp_0", "dp_1"))
    me = x * NC + c

    def remote(src, dst, send, recv, where):
        return pltpu.make_async_remote_copy(
            src_ref=src, dst_ref=dst, send_sem=send, recv_sem=recv,
            device_id=where, device_id_type=pl.DeviceIdType.MESH,
        )

    def at_xc(dx, dc):
        return lax.rem(x + dx, NX), lax.rem(c + dc, NC)

    def from_xc(dx, dc):
        return lax.rem(x + NX - dx, NX), lax.rem(c + NC - dc, NC)

    def wait(ref, sem):
        pltpu.make_async_copy(ref, ref, sem).wait()

    loads = [
        pltpu.make_async_copy(src, dst, in_sem.at[k])
        for k, (src, dst) in enumerate(
            ((up_hbm, up), (cot_hbm, cot), (w_hbm, w_own), (bias_hbm, b_own), (val_hbm, val), (gain_hbm, gain))
        )
    ]
    for load in loads:
        load.start()

    barrier = pltpu.get_barrier_semaphore()

    def greet(where):
        pl.semaphore_signal(barrier, inc=1, device_id=where, device_id_type=pl.DeviceIdType.MESH)

    for dx, dc in ORDER[1:]:
        xi, ci = at_xc(dx, dc)
        greet({"dp_0": xi, "dp_1": ci})
    for dy in range(1, NY):
        greet({"sp_1": lax.rem(y + dy, NY)})
    for dz in range(1, NZ):
        greet({"sp_0": lax.rem(z + dz, NZ)})
    swap_to = {"sp_0": lax.rem(z + me, NZ), "dp_0": z // NC, "dp_1": lax.rem(z, NC)}
    turn = lax.rem(z + NZ - me, NZ)
    stays = me + z == 0

    @pl.when(jnp.logical_not(stays))
    def _():
        greet({"sp_0": me, "dp_0": turn // NC, "dp_1": lax.rem(turn, NC)})

    def cols(i):
        return pl.ds(pl.multiple_of(i * CHUNK, CHUNK), CHUNK)

    def gate_chunk(i):
        @pl.loop(0, ROWS // 32)
        def _(t):
            rows = pl.ds(pl.multiple_of(t * 32, 32), 32)
            u = up[rows, cols(i)].astype(F32)
            u = (u * phi(u)).astype(BF16).astype(F32)
            g = (cot[rows, cols(i)].astype(F32) * u).astype(BF16)
            for k in range(NY):
                S[0, i, k, rows, :] = g[:, k * DIM : (k + 1) * DIM]

    def span(k, n):
        return pl.ds(pl.multiple_of(k * n, n), n)

    def forward(n):
        xs, cs = from_xc(*ORDER[n])
        s = xs * NC + cs
        src = S.at[0, s] if n == 0 else X.at[s]
        dst = Y.at[0, span(y, ROWS), span(s, DIM)]
        for dy in range(1, NY):
            to = lax.rem(y + dy, NY)
            remote(src.at[to], dst, yo_send, yo_recv, {"sp_1": to}).start()
        pltpu.make_async_copy(src.at[y], dst, yo_recv).start()

    def push(n):
        if n == 0:
            forward(0)
            return
        xi, ci = at_xc(*ORDER[n])
        remote(
            S.at[0, xi * NC + ci], X.at[me], xo_send, xo_recv.at[n], {"dp_0": xi, "dp_1": ci}
        ).start()

    def relay(n):
        xs, cs = from_xc(*ORDER[n])
        wait(X.at[xs * NC + cs], xo_recv.at[n])
        forward(n)

    loads[0].wait()
    loads[1].wait()
    for d in ORDER:
        xi, ci = at_xc(*d)
        gate_chunk(xi * NC + ci)

    peers = NI - 1 + NY - 1 + NZ - 1

    @pl.when(jnp.logical_not(stays))
    def _():
        pl.semaphore_wait(barrier, peers + 1)

    @pl.when(stays)
    def _():
        pl.semaphore_wait(barrier, peers)

    loads[2].wait()
    loads[3].wait()
    moves = ((w_own, w_in), (b_own, b_in))

    @pl.when(jnp.logical_not(stays))
    def _():
        for k, (src, dst) in enumerate(moves):
            remote(src, dst, sw_send.at[k], sw_recv.at[k], swap_to).start()

    @pl.when(stays)
    def _():
        for k, (src, dst) in enumerate(moves):
            pltpu.make_async_copy(src, dst, sw_recv.at[k]).start()

    for n in range(NI):
        push(n)
    loads[4].wait()
    loads[5].wait()

    @pl.loop(0, ROWS // 16)
    def _(t):
        rows = pl.ds(pl.multiple_of(t * 16, 16), 16)
        total = jnp.zeros((16, DIM), F32)
        for i in range(NI):
            v = val[rows, i * CHUNK : (i + 1) * CHUNK].astype(F32)
            v = v * phi(v)
            act[rows, i * CHUNK : (i + 1) * CHUNK] = v
            v = v * v
            for k in range(NY):
                total += v[:, k * DIM : (k + 1) * DIM]
        scale = lax.rsqrt(jnp.sum(total, axis=1, keepdims=True) / WIDTH + norm_floor)
        inv[rows, :] = jnp.broadcast_to(scale, (16, DIM))
        for i in range(NI):
            for k in range(NY):
                at = slice((i * NY + k) * DIM, (i * NY + k + 1) * DIM)
                S[1, i, k, rows, :] = (act[rows, at] * scale * gain[0:1, at]).astype(BF16)

    for dy in range(1, NY):
        to = lax.rem(y + dy, NY)
        remote(S.at[1, :, to], V.at[:, span(y, ROWS)], vy_send, vy_recv, {"sp_1": to}).start()
    pltpu.make_async_copy(S.at[1, :, y], V.at[:, span(y, ROWS)], vy_recv).start()

    def slopes(src, dst):
        @pl.loop(0, ROWS // 32 * NI)
        def _(t):
            rows = pl.ds(pl.multiple_of(t // NI * 32, 32), 32)
            at = cols(lax.rem(t, NI))
            dst[rows, at] = slope(src[rows, at].astype(F32))

    relay(1)
    slopes(up, su)

    def along(dz):
        return lax.rem(z + dz, NZ)

    def part_of(dz):
        return lax.rem(turn + dz, NZ)

    half = PART // 2
    low, high = pl.ds(0, half), pl.ds(half, half)
    wait(w_in, sw_recv.at[0])
    wait(b_in, sw_recv.at[1])
    for dz in (1, 7, 2, 6):
        remote(w_in, W.at[turn], wz_send, wz_recv.at[dz], {"sp_0": along(dz)}).start()
    pltpu.make_async_copy(w_in, W.at[turn], wz_recv.at[0]).start()
    for n in (2, 3):
        relay(n)

    for k in range(BLOCK // DIM):
        part = jnp.broadcast_to(b_in[0:1, k * DIM : (k + 1) * DIM], (DIM, DIM))
        bcol[k * DIM : (k + 1) * DIM, :] = jnp.transpose(part)

    slopes(val, sv)

    for n in (4, 5):
        relay(n)
    wait(V, vy_recv)
    for n, d in enumerate(ORDER):
        xi, ci = at_xc(*d)
        dst = Y.at[1, :, span(me, DIM)]
        if n == 0:
            pltpu.make_async_copy(V.at[me], dst, vx_recv).start()
        else:
            remote(V.at[xi * NC + ci], dst, vx_send, vx_recv, {"dp_0": xi, "dp_1": ci}).start()
    for n in (6, 7):
        relay(n)

    def pair(dx):
        return lax.rem(x + NX - dx, NX)

    def tile(t):
        return span(t, ROWS)

    for dz, on, full, part, rows in ((6, 1, 3, 4, low), (2, 7, 5, 8, high)):
        kept = part_of(dz)
        wait(W.at[kept], wz_recv.at[NZ - dz])
        remote(W.at[kept], W.at[kept], wz_send, wz_recv.at[full], {"sp_0": along(on)}).start()
        remote(
            W.at[kept, rows], W.at[kept, rows], wz_send, wz_recv.at[part], {"sp_0": along(NZ - dz)}
        ).start()

    for dz, sem in ((0, 0), (7, 1), (1, 7), (5, 3), (3, 5)):
        wait(W.at[part_of(dz)], wz_recv.at[sem])
    wait(W.at[part_of(4), low], wz_recv.at[4])
    wait(W.at[part_of(4), high], wz_recv.at[8])

    @pl.loop(0, NZ)
    def _(j):
        WT[:, pl.ds(pl.multiple_of(j * PART, PART), PART)] = jnp.transpose(W[j])

    def back(dx):
        xs = pair(dx)

        @pl.loop(0, NY)
        def _(t):
            part = jnp.dot(WT[tile(t), :], Y[0, :, span(xs, NC * DIM)], preferred_element_type=F32)
            part = part.astype(BF16)
            R0[xs, t, 0] = part[:, :DIM]
            R0[xs, t, 1] = part[:, DIM:]

        for dy in range(1, NY):
            to = lax.rem(y + dy, NY)
            remote(R0.at[xs, to], H0.at[xs, y], yr_send, yr_recv.at[dx], {"sp_1": to}).start()
        pltpu.make_async_copy(R0.at[xs, y], H0.at[xs, y], yr_recv.at[dx]).start()

    def home(dx):
        xs = pair(dx)
        wait(H0.at[xs], yr_recv.at[dx])
        for dc in range(NC):
            n = ORDER.index(((NX - dx) % NX, dc))
            cs = lax.rem(c + dc, NC)
            src, dst = H0.at[xs, :, cs], B.at[0, me]
            if n == 0:
                pltpu.make_async_copy(src, dst, xr_recv.at[n]).start()
            else:
                remote(src, dst, xr_send, xr_recv.at[n], {"dp_0": xs, "dp_1": cs}).start()

    def mixed(dx):
        xs = pair(dx)

        @pl.loop(0, NY)
        def _(t):
            rows = jnp.concatenate([W[t * 2], W[t * 2 + 1]], axis=0)
            part = jnp.dot(rows, Y[1, :, span(xs, NC * DIM)], preferred_element_type=F32)
            col = bcol[tile(t), :]
            part = (part + jnp.concatenate([col, col], axis=1)).astype(BF16)
            R1[xs * NC, t] = part[:, :DIM]
            R1[xs * NC + 1, t] = part[:, DIM:]

        for dc in range(NC):
            n = ORDER.index(((NX - dx) % NX, dc))
            cs = lax.rem(c + dc, NC)
            if n > 0:
                remote(
                    R1.at[xs * NC + cs], H1.at[me], mx_send, mx_recv.at[n], {"dp_0": xs, "dp_1": cs}
                ).start()

    def settle(n):
        xs, cs = from_xc(*ORDER[n])
        s = xs * NC + cs
        if n > 0:
            wait(H1.at[s], mx_recv.at[n])
        src = (R1 if n == 0 else H1).at[s]
        for dy in range(1, NY):
            to = lax.rem(y + dy, NY)
            remote(src.at[to], B.at[1, s, y], my_send, my_recv.at[n], {"sp_1": to}).start()
        pltpu.make_async_copy(src.at[y], B.at[1, s, y], my_recv.at[n]).start()

    def arrived(a, n):
        xs, cs = from_xc(*ORDER[n])
        s = xs * NC + cs
        wait(B.at[a, s], (my_recv if a else xr_recv).at[n])
        return s

    wait(Y.at[0], yo_recv)
    back(1)
    back(3)
    wait(Y.at[1], vx_recv)
    mixed(2)

    @pl.loop(0, NY * NY)
    def _(t):
        i, j = t // NY, lax.rem(t, NY)
        total = lax.dot_general(Y[0, tile(i), :], Y[1, tile(j), :], NT, preferred_element_type=F32)
        total = total.astype(BF16)
        ws[i * 2, :, tile(j)] = total[:PART]
        ws[i * 2 + 1, :, tile(j)] = total[PART:]

    ones = jnp.ones((8, NI * DIM), BF16)
    bsum[...] = lax.dot_general(ones, Y[0], NT, preferred_element_type=F32)
    for j in range(NZ):
        bsend[j] = bsum[:, j * DIM : (j + 1) * DIM]

    for dz in range(1, NZ):
        remote(bsend.at[part_of(dz)], br.at[z], bi_send, bi_recv, {"sp_0": along(dz)}).start()
    pltpu.make_async_copy(bsend.at[turn], br.at[z], bi_recv).start()
    far = (
        (ws.at[part_of(3)], far3.at[0], gr_recv.at[0], 1),
        (ws.at[part_of(5)], far3.at[1], gr_recv.at[1], 7),
        (ws.at[part_of(4), low], far4.at[0], gr_recv.at[2], 2),
        (ws.at[part_of(4), high], far4.at[1], gr_recv.at[3], 6),
    )
    for src, dst, sem, dz in far:
        remote(src, dst, gr_send, sem, {"sp_0": along(dz)}).start()

    mixed(1)
    back(2)
    mixed(3)
    back(0)
    mixed(0)

    gacc[...] = jnp.zeros_like(gacc)

    @pl.loop(0, NX * NY)
    def _(t):
        xs, k = t // NY, lax.rem(t, NY)
        total = gacc[...]
        for cs in range(NC):
            part = R0[xs, k, cs].astype(F32) * Y[1, tile(k), span(xs * NC + cs, DIM)].astype(F32)
            total += jnp.sum(part.reshape(ROWS // 8, 8, DIM), axis=0)
        gacc[...] = total

    mine = pl.ds(pl.multiple_of((me * NY + y) * DIM, DIM), DIM)
    line = jnp.sum(gacc[...], axis=0, keepdims=True) / gain[0:1, mine]
    gsend[...] = jnp.broadcast_to(line, (8, DIM))
    for dz in range(1, NZ):
        remote(gsend, gz.at[z], gn_send.at[0], gn_recv.at[0], {"sp_0": along(dz)}).start()
    pltpu.make_async_copy(gsend, gz.at[z], gn_recv.at[0]).start()

    home(1)
    settle(6)
    settle(7)
    home(3)

    for k, (dz, rows) in enumerate(((2, low), (6, high))):
        wait(far3.at[k], gr_recv.at[k])
        wait(far4.at[k], gr_recv.at[2 + k])
        to = part_of(dz)
        ws[to] = (ws[to].astype(F32) + far3[k].astype(F32)).astype(BF16)
        ws[to, rows] = (ws[to, rows].astype(F32) + far4[k].astype(F32)).astype(BF16)
        remote(ws.at[to], wr.at[2 + k], gr_send, gr_recv.at[6 + k], {"sp_0": along(dz)}).start()

    for k, dz in enumerate((1, 7)):
        remote(ws.at[part_of(dz)], wr.at[k], gr_send, gr_recv.at[4 + k], {"sp_0": along(dz)}).start()

    wait(gz, gn_recv.at[0])
    gxs[...] = jnp.sum(gz[...], axis=0)
    for n, d in enumerate(ORDER):
        xi, ci = at_xc(*d)
        if n == 0:
            pltpu.make_async_copy(gxs, gx.at[me], gn_recv.at[1]).start()
        else:
            remote(gxs, gx.at[me], gn_send.at[1], gn_recv.at[1], {"dp_0": xi, "dp_1": ci}).start()

    home(2)
    for dc in range(NC):
        settle(ORDER.index((3, dc)))
    for dc in range(NC):
        settle(ORDER.index((1, dc)))
    home(0)
    settle(1)
    settle(0)

    def finish_gain():
        wait(gx, gn_recv.at[1])
        for i in range(NI):
            gys[i : i + 1, :] = gx[i, 0:1, :]
        for dy in range(1, NY):
            remote(gys, gy.at[y], gn_send.at[2], gn_recv.at[2], {"sp_1": lax.rem(y + dy, NY)}).start()
        pltpu.make_async_copy(gys, gy.at[y], gn_recv.at[2]).start()

    dot[...] = jnp.zeros_like(dot)

    def row_sums(n):
        s = arrived(0, n)

        @pl.loop(0, ROWS // 32)
        def _(t):
            rows = pl.ds(pl.multiple_of(t * 32, 32), 32)
            total = dot[rows, :]
            for k in range(NY):
                at = pl.ds(pl.multiple_of((s * NY + k) * DIM, DIM), DIM)
                total += B[0, s, k, rows, :].astype(F32) * gain[0:1, at] * act[rows, at]
            dot[rows, :] = total

    for n in (2, 3, 4, 5):
        row_sums(n)

    for k in range(4):
        wait(wr.at[k], gr_recv.at[4 + k])
    wait(br, bi_recv)

    @pl.loop(0, PART // 16)
    def _(t):
        rows = pl.ds(pl.multiple_of(t * 16, 16), 16)
        total = ws[turn, rows, :].astype(F32)
        for k in range(4):
            total += wr[k, rows, :].astype(F32)
        wsum[rows, :] = total.astype(BF16)

    bsum[:, :DIM] = jnp.sum(br[...], axis=0)
    first = ((wsum, wmid), (bsum.at[:, pl.ds(0, DIM)], bmid))
    second = ((wmid, wout), (bmid, bout))

    @pl.when(turn != me)
    def _():
        for k, (src, dst) in enumerate(first):
            remote(
                src, dst, so_send.at[k], so_recv.at[k], {"dp_0": turn // NC, "dp_1": lax.rem(turn, NC)}
            ).start()

    @pl.when(turn == me)
    def _():
        for k, (src, dst) in enumerate(first):
            pltpu.make_async_copy(src, dst, so_recv.at[k]).start()

    for n in (6, 7, 1, 0):
        row_sums(n)

    wait(wmid, so_recv.at[0])
    wait(bmid, so_recv.at[1])

    @pl.when(me != 0)
    def _():
        for k, (src, dst) in enumerate(second):
            remote(src, dst, so_send.at[2 + k], so_recv.at[2 + k], {"sp_0": turn}).start()

    @pl.when(me == 0)
    def _():
        for k, (src, dst) in enumerate(second):
            pltpu.make_async_copy(src, dst, so_recv.at[2 + k]).start()

    @pl.loop(0, ROWS // 16)
    def _(t):
        rows = pl.ds(pl.multiple_of(t * 16, 16), 16)
        scale = inv[rows, :]
        mean = jnp.sum(dot[rows, :], axis=1, keepdims=True) / WIDTH
        cube = scale * scale * scale * mean
        for g in range(NI * NY):
            at = slice(g * DIM, (g + 1) * DIM)
            scaled = B[0, g // NY, g % NY, rows, :].astype(F32) * gain[0:1, at]
            grad = (scale * scaled - cube * act[rows, at]) * sv[rows, at]
            val[rows, at] = grad.astype(BF16)

    pltpu.make_async_copy(val, valg_hbm, out_sem.at[0]).start()

    def finish(n):
        s = arrived(1, n)

        @pl.loop(0, ROWS // 32)
        def _(t):
            rows = pl.ds(pl.multiple_of(t * 32, 32), 32)
            for k in range(NY):
                at = pl.ds(pl.multiple_of((s * NY + k) * DIM, DIM), DIM)
                mid = (cot[rows, at].astype(F32) * B[1, s, k, rows, :].astype(F32)).astype(BF16)
                up[rows, at] = (mid.astype(F32) * su[rows, at]).astype(BF16)

        pltpu.make_async_copy(up.at[:, cols(s)], upg_hbm.at[:, cols(s)], out_sem.at[1]).start()

    for n in (2, 3):
        finish(n)
    finish_gain()
    for n in (4, 5, 6, 7, 1, 0):
        finish(n)

    wait(gy, gn_recv.at[2])
    for i in range(NI):
        for k in range(NY):
            gall[i * NY + k : i * NY + k + 1, :] = gy[k, i : i + 1, :]
    tail = [pltpu.make_async_copy(gall, gg_hbm, out_sem.at[2])]
    tail[0].start()
    wait(wout, so_recv.at[2])
    wait(bout, so_recv.at[3])
    wfin[...] = wout[...].astype(F32)
    tail += [
        pltpu.make_async_copy(wfin, wg_hbm, out_sem.at[3]),
        pltpu.make_async_copy(bout, bg_hbm, out_sem.at[4]),
    ]
    for copy in tail[1:]:
        copy.start()

    wait(X.at[pl.ds(0, NI - 1)], xo_send)
    wait(X.at[:, pl.ds(0, NY - 1)], yo_send)
    wait(S.at[1, :, pl.ds(0, NY - 1)], vy_send)
    wait(V.at[pl.ds(0, NI - 1)], vx_send)
    wait(R0.at[:, pl.ds(0, NY - 1)], yr_send)
    wait(B.at[0, pl.ds(0, NI - 1)], xr_send)
    wait(H1.at[pl.ds(0, NI - 1)], mx_send)
    wait(B.at[1, :, pl.ds(0, NY - 1)], my_send)
    wait(W.at[pl.ds(0, NZ - 1)], wz_send)
    wait(ws.at[pl.ds(0, NZ - 1)], gr_send)
    wait(bsend.at[pl.ds(0, NZ - 1)], bi_send)
    wait(gz.at[pl.ds(0, NZ - 1)], gn_send.at[0])
    wait(gx.at[pl.ds(0, NI - 1)], gn_send.at[1])
    wait(gy.at[pl.ds(0, NY - 1)], gn_send.at[2])

    @pl.when(jnp.logical_not(stays))
    def _():
        for k, (src, dst) in enumerate(moves):
            wait(src, sw_send.at[k])

    @pl.when(turn != me)
    def _():
        for k, (src, dst) in enumerate(first):
            wait(src, so_send.at[k])

    @pl.when(me != 0)
    def _():
        for k, (src, dst) in enumerate(second):
            wait(src, so_send.at[2 + k])

    wait(val, out_sem.at[0])
    wait(up, out_sem.at[1])
    for copy in tail:
        copy.wait()


def shards(cotangent, up_pre, value_pre, spatial_weight, spatial_bias, value_gain):
    vmem, dma = pltpu.VMEM, pltpu.SemaphoreType.DMA
    tok = (ROWS, WIDTH)
    out = pl.pallas_call(
        kernel,
        name="gating_backward",
        out_shape=(
            jax.ShapeDtypeStruct(tok, BF16),
            jax.ShapeDtypeStruct(tok, BF16),
            jax.ShapeDtypeStruct((PART, BLOCK), F32),
            jax.ShapeDtypeStruct((8, DIM), F32),
            jax.ShapeDtypeStruct((NY * NI, DIM), F32),
        ),
        in_specs=[pl.BlockSpec(memory_space=pl.ANY)] * 6,
        out_specs=[pl.BlockSpec(memory_space=pl.ANY)] * 5,
        scratch_shapes=[
            vmem(tok, BF16), vmem(tok, BF16), vmem(tok, BF16),
            vmem((PART, BLOCK), BF16), vmem((1, BLOCK), F32), vmem((1, WIDTH), F32),
            vmem((2, NI, NY, ROWS, DIM), BF16),
            vmem((NI, NY, ROWS, DIM), BF16),
            vmem((NI, BLOCK, DIM), BF16),
            vmem((2, BLOCK, NI * DIM), BF16),
            vmem((NX, NY, NC, ROWS, DIM), BF16), vmem((NI, NY, ROWS, DIM), BF16),
            vmem((NX, NY, NC, ROWS, DIM), BF16), vmem((NI, NY, ROWS, DIM), BF16),
            vmem((2, NI, NY, ROWS, DIM), BF16),
            vmem((PART, BLOCK), BF16), vmem((1, BLOCK), F32),
            vmem((NZ, PART, BLOCK), BF16), vmem((BLOCK, BLOCK), BF16), vmem((BLOCK, DIM), F32),
            vmem((NZ, PART, BLOCK), BF16), vmem((4, PART, BLOCK), BF16),
            vmem((2, PART, BLOCK), BF16), vmem((2, PART // 2, BLOCK), BF16),
            vmem((PART, BLOCK), BF16), vmem((PART, BLOCK), BF16), vmem((PART, BLOCK), BF16),
            vmem((PART, BLOCK), F32),
            vmem((NZ, 8, DIM), F32), vmem((NZ, 8, DIM), F32), vmem((8, BLOCK), F32),
            vmem((8, DIM), F32), vmem((8, DIM), F32),
            vmem((8, DIM), F32), vmem((NZ, 8, DIM), F32), vmem((8, DIM), F32), vmem((NI, 8, DIM), F32),
            vmem((NI, DIM), F32), vmem((NY, NI, DIM), F32), vmem((NY * NI, DIM), F32),
            vmem(tok, F32), vmem(tok, F32), vmem(tok, F32),
            vmem((ROWS, DIM), F32), vmem((ROWS, DIM), F32), vmem((8, DIM), F32),
            dma((6,)), dma((5,)),
            dma(()), dma((NI,)), dma(()), dma(()), dma(()), dma(()), dma(()), dma(()),
            dma((2,)), dma((2,)), dma(()), dma((9,)),
            dma(()), dma((NX,)), dma(()), dma((NI,)), dma(()), dma((NI,)), dma(()), dma((NI,)),
            dma(()), dma((8,)), dma(()), dma(()), dma((4,)), dma((4,)),
            dma((3,)), dma((3,)),
        ],
        compiler_params=pltpu.CompilerParams(
            collective_id=0, has_side_effects=True, vmem_limit_bytes=67043328
        ),
    )(
        cotangent[0], up_pre[0], value_pre[0], spatial_weight[0], spatial_bias, value_gain[None]
    )
    up_grad, value_grad, weight_grad, bias_grad, gain_grad = out
    return up_grad[None], value_grad[None], weight_grad[None], bias_grad[:1], gain_grad.reshape(WIDTH)


def solution(mesh):
    torus = Mesh(mesh.devices.reshape(NZ, NY, NX, NC), ("sp_0", "sp_1", "dp_0", "dp_1"))
    in_specs = (
        P(DP, SP, None),
        P(DP, SP, None),
        P(DP, SP, None),
        P(SP, DP, None),
        P(SP, None),
        P(),
    )
    out_specs = (P(DP, SP, None), P(DP, SP, None), P(SP, DP, None), P(SP, DP), P())
    return jax.shard_map(
        shards, mesh=torus, in_specs=in_specs, out_specs=out_specs, check_vma=False
    )
```

time: 208 us -> 142 us (0.68)
  the two profiles are of different devices: /device:TPU:89 before, /device:TPU:69 now
where the time goes in v3:
time: 142 us
  Pallas kernels  134 us (94%)
  local copies, waits for them, and re-layouts  7.25 us (5%)
    pallas_call x1, Pallas kernels, shards(): pl.pallas_call(kernel, name='gating_backward', out_shape=(jax.ShapeDtypeS...  134 us
    unnamed x10, local copies, waits for them, and re-layouts  6.05 us

profile of v3, /device:TPU:69, one launch (start us, length us, event | category | flops | bytes accessed | tf_op | source)
XLA Modules:
  0.0 142.1 jit_solution(1432893990712907025)
XLA Ops:
  0.6 134.2 %gating_backward.1 = (bf16[256,4096]{1,0:T(8,128)(2,1)}, bf16[256,4096]{1,0:T(8,128)(2,1)}, f32[128,1024]{1,0:T(8,128)}, f32[8,128]{1,0:T(8,128)}, f32[32,128]{1,0:T(8,128)}) custom-call(bf16[256,4096]{1,0:T(8,128)(2,1)} %bitcast.11, bf16[256,4096]{1,0:T(8,128)(2,1)} %bitcast.12, bf16[256,4096]{1,0:T(8,128)(2,1)} %bitcast.13, bf16[128,1024]{1,0:T(8,128)(2,1)} %bitcast.15, ...), custom_call_target="tpu_custom_call" | custom-call | tf_op jit(solution)/shard_map/gating_backward/pallas_call | solution.py:579
  134.8 1.2 slice.3
  136.0 0.0 copy-start
  136.0 3.3 %copy.15 = bf16[1,256,4096]{2,1,0:T(8,128)(2,1)} copy(bf16[1,256,4096]{2,1,0:T(8,128)(2,1)} %bitcast.10) | data formatting | bytes 4194304
  139.3 0.0 copy-done
  139.3 0.0 copy-start.1
  139.3 0.0 copy-start.2
  139.3 1.3 copy.16
  140.6 0.1 copy-done.1
  140.7 0.8 copy.17
  141.5 0.0 copy-done.2
  141.5 0.6 copy.18
Async XLA Ops:
  136.0 3.3 %copy-start = (bf16[256,4096]{1,0:T(8,128)(2,1)S(1)}, bf16[256,4096]{1,0:T(8,128)(2,1)}, u32[]{:S(2)}) copy-start(bf16[256,4096]{1,0:T(8,128)(2,1)} %get-tuple-element.11) | copy-start | bytes 6291460
  139.3 1.4 copy-start.1
  139.3 2.2 %copy-start.2 = (f32[32,128]{1,0:T(8,128)S(1)}, f32[32,128]{1,0:T(8,128)}, u32[]{:S(2)}) copy-start(f32[32,128]{1,0:T(8,128)} %get-tuple-element.14) | copy-start | bytes 49156

commit v4 on v3

--- a/solution.py
+++ b/solution.py
@@ -39,14 +39,14 @@
 
 def kernel(
     cot_hbm, up_hbm, val_hbm, w_hbm, bias_hbm, gain_hbm,
-    upg_hbm, valg_hbm, wg_hbm, bg_hbm, gg_hbm,
+    upg, valg, wout, bout, gall,
     cot, up, val, w_own, b_own, gain,
     S, X, V, Y, R0, R1, H0, H1, B,
     w_in, b_in, W, WT, bcol,
-    ws, wr, far3, far4, wsum, wmid, wout, wfin, bsend, br, bsum, bmid, bout,
-    gsend, gz, gxs, gx, gys, gy, gall,
+    ws, wr, far3, far4, wsum, wmid, bsend, br, bsum, bmid,
+    gsend, gz, gxs, gx, gys, gy,
     act, su, sv, inv, dot, gacc,
-    in_sem, out_sem,
+    in_sem,
     xo_send, xo_recv, yo_send, yo_recv, vy_send, vy_recv, vx_send, vx_recv,
     sw_send, sw_recv, wz_send, wz_recv,
     yr_send, yr_recv, xr_send, xr_recv, mx_send, mx_recv, my_send, my_recv,
@@ -77,8 +77,8 @@
             ((up_hbm, up), (cot_hbm, cot), (w_hbm, w_own), (bias_hbm, b_own), (val_hbm, val), (gain_hbm, gain))
         )
     ]
-    for load in loads:
-        load.start()
+    for k in (4, 5, 2, 3, 0, 1):
+        loads[k].start()
 
     barrier = pltpu.get_barrier_semaphore()
 
@@ -92,13 +92,22 @@
         greet({"sp_1": lax.rem(y + dy, NY)})
     for dz in range(1, NZ):
         greet({"sp_0": lax.rem(z + dz, NZ)})
-    swap_to = {"sp_0": lax.rem(z + me, NZ), "dp_0": z // NC, "dp_1": lax.rem(z, NC)}
+    shift = x + c * NX
+    swap_to = {"sp_0": lax.rem(z + shift, NZ), "dp_0": z // NC, "dp_1": lax.rem(z, NC)}
     turn = lax.rem(z + NZ - me, NZ)
+
+    def part_of(dz):
+        t = lax.rem(turn + dz, NZ)
+        return lax.rem(t, NX) * NC + t // NX
+
+    mine = part_of(0)
+    swap_from = {"sp_0": me, "dp_0": mine // NC, "dp_1": lax.rem(mine, NC)}
     stays = me + z == 0
 
     @pl.when(jnp.logical_not(stays))
     def _():
-        greet({"sp_0": me, "dp_0": turn // NC, "dp_1": lax.rem(turn, NC)})
+        greet(swap_from)
+        greet(swap_to)
 
     def cols(i):
         return pl.ds(pl.multiple_of(i * CHUNK, CHUNK), CHUNK)
@@ -127,9 +136,6 @@
         pltpu.make_async_copy(src.at[y], dst, yo_recv).start()
 
     def push(n):
-        if n == 0:
-            forward(0)
-            return
         xi, ci = at_xc(*ORDER[n])
         remote(
             S.at[0, xi * NC + ci], X.at[me], xo_send, xo_recv.at[n], {"dp_0": xi, "dp_1": ci}
@@ -140,38 +146,6 @@
         wait(X.at[xs * NC + cs], xo_recv.at[n])
         forward(n)
 
-    loads[0].wait()
-    loads[1].wait()
-    for d in ORDER:
-        xi, ci = at_xc(*d)
-        gate_chunk(xi * NC + ci)
-
-    peers = NI - 1 + NY - 1 + NZ - 1
-
-    @pl.when(jnp.logical_not(stays))
-    def _():
-        pl.semaphore_wait(barrier, peers + 1)
-
-    @pl.when(stays)
-    def _():
-        pl.semaphore_wait(barrier, peers)
-
-    loads[2].wait()
-    loads[3].wait()
-    moves = ((w_own, w_in), (b_own, b_in))
-
-    @pl.when(jnp.logical_not(stays))
-    def _():
-        for k, (src, dst) in enumerate(moves):
-            remote(src, dst, sw_send.at[k], sw_recv.at[k], swap_to).start()
-
-    @pl.when(stays)
-    def _():
-        for k, (src, dst) in enumerate(moves):
-            pltpu.make_async_copy(src, dst, sw_recv.at[k]).start()
-
-    for n in range(NI):
-        push(n)
     loads[4].wait()
     loads[5].wait()
 
@@ -193,10 +167,48 @@
                 at = slice((i * NY + k) * DIM, (i * NY + k + 1) * DIM)
                 S[1, i, k, rows, :] = (act[rows, at] * scale * gain[0:1, at]).astype(BF16)
 
+    peers = NI - 1 + NY - 1 + NZ - 1
+
+    @pl.when(jnp.logical_not(stays))
+    def _():
+        pl.semaphore_wait(barrier, peers + 2)
+
+    @pl.when(stays)
+    def _():
+        pl.semaphore_wait(barrier, peers)
+
+    loads[2].wait()
+    loads[3].wait()
+    moves = ((w_own, w_in), (b_own, b_in))
+
+    def quarters(src, dst, send, recv, where):
+        for k in range(4):
+            rows = pl.ds(k * (PART // 4), PART // 4)
+            remote(src.at[rows], dst.at[rows], send, recv, where).start()
+
+    @pl.when(jnp.logical_not(stays))
+    def _():
+        quarters(w_own, w_in, sw_send.at[0], sw_recv.at[0], swap_to)
+        remote(b_own, b_in, sw_send.at[1], sw_recv.at[1], swap_to).start()
+
+    @pl.when(stays)
+    def _():
+        for k, (src, dst) in enumerate(moves):
+            pltpu.make_async_copy(src, dst, sw_recv.at[k]).start()
+
     for dy in range(1, NY):
         to = lax.rem(y + dy, NY)
         remote(S.at[1, :, to], V.at[:, span(y, ROWS)], vy_send, vy_recv, {"sp_1": to}).start()
     pltpu.make_async_copy(S.at[1, :, y], V.at[:, span(y, ROWS)], vy_recv).start()
+
+    loads[0].wait()
+    loads[1].wait()
+    for n, d in enumerate(ORDER):
+        xi, ci = at_xc(*d)
+        gate_chunk(xi * NC + ci)
+        if n > 1:
+            push(n - 1)
+    push(NI - 1)
 
     def slopes(src, dst):
         @pl.loop(0, ROWS // 32 * NI)
@@ -205,24 +217,18 @@
             at = cols(lax.rem(t, NI))
             dst[rows, at] = slope(src[rows, at].astype(F32))
 
-    relay(1)
     slopes(up, su)
 
     def along(dz):
         return lax.rem(z + dz, NZ)
-
-    def part_of(dz):
-        return lax.rem(turn + dz, NZ)
 
     half = PART // 2
     low, high = pl.ds(0, half), pl.ds(half, half)
     wait(w_in, sw_recv.at[0])
     wait(b_in, sw_recv.at[1])
     for dz in (1, 7, 2, 6):
-        remote(w_in, W.at[turn], wz_send, wz_recv.at[dz], {"sp_0": along(dz)}).start()
-    pltpu.make_async_copy(w_in, W.at[turn], wz_recv.at[0]).start()
-    for n in (2, 3):
-        relay(n)
+        remote(w_in, W.at[mine], wz_send, wz_recv.at[dz], {"sp_0": along(dz)}).start()
+    pltpu.make_async_copy(w_in, W.at[mine], wz_recv.at[0]).start()
 
     for k in range(BLOCK // DIM):
         part = jnp.broadcast_to(b_in[0:1, k * DIM : (k + 1) * DIM], (DIM, DIM))
@@ -230,17 +236,18 @@
 
     slopes(val, sv)
 
-    for n in (4, 5):
-        relay(n)
     wait(V, vy_recv)
     for n, d in enumerate(ORDER):
         xi, ci = at_xc(*d)
         dst = Y.at[1, :, span(me, DIM)]
         if n == 0:
-            pltpu.make_async_copy(V.at[me], dst, vx_recv).start()
+            pltpu.make_async_copy(V.at[me], dst, vx_recv.at[d[0]]).start()
         else:
-            remote(V.at[xi * NC + ci], dst, vx_send, vx_recv, {"dp_0": xi, "dp_1": ci}).start()
-    for n in (6, 7):
+            remote(V.at[xi * NC + ci], dst, vx_send, vx_recv.at[d[0]], {"dp_0": xi, "dp_1": ci}).start()
+    for n in (2, 3, 4, 5):
+        relay(n)
+    forward(0)
+    for n in (1, 6, 7):
         relay(n)
 
     def pair(dx):
@@ -261,10 +268,6 @@
         wait(W.at[part_of(dz)], wz_recv.at[sem])
     wait(W.at[part_of(4), low], wz_recv.at[4])
     wait(W.at[part_of(4), high], wz_recv.at[8])
-
-    @pl.loop(0, NZ)
-    def _(j):
-        WT[:, pl.ds(pl.multiple_of(j * PART, PART), PART)] = jnp.transpose(W[j])
 
     def back(dx):
         xs = pair(dx)
@@ -330,42 +333,54 @@
         wait(B.at[a, s], (my_recv if a else xr_recv).at[n])
         return s
 
+    def value_pair(dx):
+        wait(Y.at[1, :, span(pair(dx), NC * DIM)], vx_recv.at[dx])
+
+    def outer(p, q):
+        p, q = part_of(p), part_of(q)
+
+        @pl.loop(0, NY)
+        def _(j):
+            rows = jnp.concatenate([Y[0, span(p, PART), :], Y[0, span(q, PART), :]], axis=0)
+            total = lax.dot_general(rows, Y[1, tile(j), :], NT, preferred_element_type=F32).astype(BF16)
+            ws[p, :, tile(j)] = total[:PART]
+            ws[q, :, tile(j)] = total[PART:]
+
+    value_pair(1)
+    mixed(1)
+    value_pair(3)
+    mixed(3)
+
+    @pl.loop(0, NZ)
+    def _(j):
+        WT[:, pl.ds(pl.multiple_of(j * PART, PART), PART)] = jnp.transpose(W[j])
+
     wait(Y.at[0], yo_recv)
     back(1)
+    value_pair(2)
+    value_pair(0)
+
+    outer(3, 5)
+    remote(ws.at[part_of(3)], far3.at[0], gr_send, gr_recv.at[0], {"sp_0": along(1)}).start()
+    remote(ws.at[part_of(5)], far3.at[1], gr_send, gr_recv.at[1], {"sp_0": along(7)}).start()
+    outer(4, 2)
+    remote(ws.at[part_of(4), low], far4.at[0], gr_send, gr_recv.at[2], {"sp_0": along(2)}).start()
+    remote(ws.at[part_of(4), high], far4.at[1], gr_send, gr_recv.at[3], {"sp_0": along(6)}).start()
     back(3)
-    wait(Y.at[1], vx_recv)
     mixed(2)
-
-    @pl.loop(0, NY * NY)
-    def _(t):
-        i, j = t // NY, lax.rem(t, NY)
-        total = lax.dot_general(Y[0, tile(i), :], Y[1, tile(j), :], NT, preferred_element_type=F32)
-        total = total.astype(BF16)
-        ws[i * 2, :, tile(j)] = total[:PART]
-        ws[i * 2 + 1, :, tile(j)] = total[PART:]
+    back(2)
+    outer(6, 1)
+    outer(7, 0)
 
     ones = jnp.ones((8, NI * DIM), BF16)
     bsum[...] = lax.dot_general(ones, Y[0], NT, preferred_element_type=F32)
     for j in range(NZ):
         bsend[j] = bsum[:, j * DIM : (j + 1) * DIM]
-
+    back(0)
+    mixed(0)
     for dz in range(1, NZ):
         remote(bsend.at[part_of(dz)], br.at[z], bi_send, bi_recv, {"sp_0": along(dz)}).start()
-    pltpu.make_async_copy(bsend.at[turn], br.at[z], bi_recv).start()
-    far = (
-        (ws.at[part_of(3)], far3.at[0], gr_recv.at[0], 1),
-        (ws.at[part_of(5)], far3.at[1], gr_recv.at[1], 7),
-        (ws.at[part_of(4), low], far4.at[0], gr_recv.at[2], 2),
-        (ws.at[part_of(4), high], far4.at[1], gr_recv.at[3], 6),
-    )
-    for src, dst, sem, dz in far:
-        remote(src, dst, gr_send, sem, {"sp_0": along(dz)}).start()
-
-    mixed(1)
-    back(2)
-    mixed(3)
-    back(0)
-    mixed(0)
+    pltpu.make_async_copy(bsend.at[mine], br.at[z], bi_recv).start()
 
     gacc[...] = jnp.zeros_like(gacc)
 
@@ -378,16 +393,13 @@
             total += jnp.sum(part.reshape(ROWS // 8, 8, DIM), axis=0)
         gacc[...] = total
 
-    mine = pl.ds(pl.multiple_of((me * NY + y) * DIM, DIM), DIM)
-    line = jnp.sum(gacc[...], axis=0, keepdims=True) / gain[0:1, mine]
+    line = jnp.sum(gacc[...], axis=0, keepdims=True) / gain[0:1, span(me * NY + y, DIM)]
     gsend[...] = jnp.broadcast_to(line, (8, DIM))
     for dz in range(1, NZ):
         remote(gsend, gz.at[z], gn_send.at[0], gn_recv.at[0], {"sp_0": along(dz)}).start()
     pltpu.make_async_copy(gsend, gz.at[z], gn_recv.at[0]).start()
 
     home(1)
-    settle(6)
-    settle(7)
     home(3)
 
     for k, (dz, rows) in enumerate(((2, low), (6, high))):
@@ -400,6 +412,17 @@
 
     for k, dz in enumerate((1, 7)):
         remote(ws.at[part_of(dz)], wr.at[k], gr_send, gr_recv.at[4 + k], {"sp_0": along(dz)}).start()
+
+    for dx in (3, 1):
+        for dc in range(NC):
+            settle(ORDER.index((dx, dc)))
+    home(2)
+
+    settle(1)
+    settle(0)
+    home(0)
+    settle(6)
+    settle(7)
 
     wait(gz, gn_recv.at[0])
     gxs[...] = jnp.sum(gz[...], axis=0)
@@ -410,15 +433,6 @@
         else:
             remote(gxs, gx.at[me], gn_send.at[1], gn_recv.at[1], {"dp_0": xi, "dp_1": ci}).start()
 
-    home(2)
-    for dc in range(NC):
-        settle(ORDER.index((3, dc)))
-    for dc in range(NC):
-        settle(ORDER.index((1, dc)))
-    home(0)
-    settle(1)
-    settle(0)
-
     def finish_gain():
         wait(gx, gn_recv.at[1])
         for i in range(NI):
@@ -426,6 +440,17 @@
         for dy in range(1, NY):
             remote(gys, gy.at[y], gn_send.at[2], gn_recv.at[2], {"sp_1": lax.rem(y + dy, NY)}).start()
         pltpu.make_async_copy(gys, gy.at[y], gn_recv.at[2]).start()
+
+    def finish(n):
+        s = arrived(1, n)
+
+        @pl.loop(0, ROWS // 32)
+        def _(t):
+            rows = pl.ds(pl.multiple_of(t * 32, 32), 32)
+            for k in range(NY):
+                at = pl.ds(pl.multiple_of((s * NY + k) * DIM, DIM), DIM)
+                mid = (cot[rows, at].astype(F32) * B[1, s, k, rows, :].astype(F32)).astype(BF16)
+                upg[rows, at] = (mid.astype(F32) * su[rows, at]).astype(BF16)
 
     dot[...] = jnp.zeros_like(dot)
 
@@ -441,7 +466,7 @@
                 total += B[0, s, k, rows, :].astype(F32) * gain[0:1, at] * act[rows, at]
             dot[rows, :] = total
 
-    for n in (2, 3, 4, 5):
+    for n in (2, 3):
         row_sums(n)
 
     for k in range(4):
@@ -451,29 +476,41 @@
     @pl.loop(0, PART // 16)
     def _(t):
         rows = pl.ds(pl.multiple_of(t * 16, 16), 16)
-        total = ws[turn, rows, :].astype(F32)
+        total = ws[mine, rows, :].astype(F32)
         for k in range(4):
             total += wr[k, rows, :].astype(F32)
         wsum[rows, :] = total.astype(BF16)
 
     bsum[:, :DIM] = jnp.sum(br[...], axis=0)
-    first = ((wsum, wmid), (bsum.at[:, pl.ds(0, DIM)], bmid))
-    second = ((wmid, wout), (bmid, bout))
-
-    @pl.when(turn != me)
-    def _():
+    first = ((wsum.at[low], wmid), (bsum.at[:, pl.ds(0, DIM)], bmid))
+    second = ((wmid, wout.at[low]), (bmid, bout))
+
+    @pl.when(jnp.logical_not(stays))
+    def _():
+        remote(wsum.at[high], wout.at[high], so_send.at[4], so_recv.at[4], swap_from).start()
+
+    @pl.when(stays)
+    def _():
+        pltpu.make_async_copy(wsum.at[high], wout.at[high], so_recv.at[4]).start()
+
+    @pl.when(mine != me)
+    def _():
+        where = {"dp_0": mine // NC, "dp_1": lax.rem(mine, NC)}
         for k, (src, dst) in enumerate(first):
-            remote(
-                src, dst, so_send.at[k], so_recv.at[k], {"dp_0": turn // NC, "dp_1": lax.rem(turn, NC)}
-            ).start()
-
-    @pl.when(turn == me)
+            remote(src, dst, so_send.at[k], so_recv.at[k], where).start()
+
+    @pl.when(mine == me)
     def _():
         for k, (src, dst) in enumerate(first):
             pltpu.make_async_copy(src, dst, so_recv.at[k]).start()
 
-    for n in (6, 7, 1, 0):
+    for n in (4, 5):
         row_sums(n)
+    for n in (2, 3, 4, 5):
+        finish(n)
+    for n in (6, 7):
+        row_sums(n)
+    finish_gain()
 
     wait(wmid, so_recv.at[0])
     wait(bmid, so_recv.at[1])
@@ -481,12 +518,15 @@
     @pl.when(me != 0)
     def _():
         for k, (src, dst) in enumerate(second):
-            remote(src, dst, so_send.at[2 + k], so_recv.at[2 + k], {"sp_0": turn}).start()
+            remote(src, dst, so_send.at[2 + k], so_recv.at[2 + k], {"sp_0": lax.rem(z + NZ - shift, NZ)}).start()
 
     @pl.when(me == 0)
     def _():
         for k, (src, dst) in enumerate(second):
             pltpu.make_async_copy(src, dst, so_recv.at[2 + k]).start()
+
+    for n in (1, 0):
+        row_sums(n)
 
     @pl.loop(0, ROWS // 16)
     def _(t):
@@ -498,44 +538,18 @@
             at = slice(g * DIM, (g + 1) * DIM)
             scaled = B[0, g // NY, g % NY, rows, :].astype(F32) * gain[0:1, at]
             grad = (scale * scaled - cube * act[rows, at]) * sv[rows, at]
-            val[rows, at] = grad.astype(BF16)
-
-    pltpu.make_async_copy(val, valg_hbm, out_sem.at[0]).start()
-
-    def finish(n):
-        s = arrived(1, n)
-
-        @pl.loop(0, ROWS // 32)
-        def _(t):
-            rows = pl.ds(pl.multiple_of(t * 32, 32), 32)
-            for k in range(NY):
-                at = pl.ds(pl.multiple_of((s * NY + k) * DIM, DIM), DIM)
-                mid = (cot[rows, at].astype(F32) * B[1, s, k, rows, :].astype(F32)).astype(BF16)
-                up[rows, at] = (mid.astype(F32) * su[rows, at]).astype(BF16)
-
-        pltpu.make_async_copy(up.at[:, cols(s)], upg_hbm.at[:, cols(s)], out_sem.at[1]).start()
-
-    for n in (2, 3):
-        finish(n)
-    finish_gain()
-    for n in (4, 5, 6, 7, 1, 0):
+            valg[rows, at] = grad.astype(BF16)
+
+    for n in (6, 7, 1, 0):
         finish(n)
 
     wait(gy, gn_recv.at[2])
     for i in range(NI):
         for k in range(NY):
             gall[i * NY + k : i * NY + k + 1, :] = gy[k, i : i + 1, :]
-    tail = [pltpu.make_async_copy(gall, gg_hbm, out_sem.at[2])]
-    tail[0].start()
-    wait(wout, so_recv.at[2])
+    wait(wout.at[low], so_recv.at[2])
+    wait(wout.at[high], so_recv.at[4])
     wait(bout, so_recv.at[3])
-    wfin[...] = wout[...].astype(F32)
-    tail += [
-        pltpu.make_async_copy(wfin, wg_hbm, out_sem.at[3]),
-        pltpu.make_async_copy(bout, bg_hbm, out_sem.at[4]),
-    ]
-    for copy in tail[1:]:
-        copy.start()
 
     wait(X.at[pl.ds(0, NI - 1)], xo_send)
     wait(X.at[:, pl.ds(0, NY - 1)], yo_send)
@@ -556,8 +570,9 @@
     def _():
         for k, (src, dst) in enumerate(moves):
             wait(src, sw_send.at[k])
-
-    @pl.when(turn != me)
+        wait(wsum.at[high], so_send.at[4])
+
+    @pl.when(mine != me)
     def _():
         for k, (src, dst) in enumerate(first):
             wait(src, so_send.at[k])
@@ -566,11 +581,6 @@
     def _():
         for k, (src, dst) in enumerate(second):
             wait(src, so_send.at[2 + k])
-
-    wait(val, out_sem.at[0])
-    wait(up, out_sem.at[1])
-    for copy in tail:
-        copy.wait()
 
 
 def shards(cotangent, up_pre, value_pre, spatial_weight, spatial_bias, value_gain):
@@ -580,14 +590,14 @@
         kernel,
         name="gating_backward",
         out_shape=(
-            jax.ShapeDtypeStruct(tok, BF16),
-            jax.ShapeDtypeStruct(tok, BF16),
-            jax.ShapeDtypeStruct((PART, BLOCK), F32),
-            jax.ShapeDtypeStruct((8, DIM), F32),
-            jax.ShapeDtypeStruct((NY * NI, DIM), F32),
+            vmem(tok, BF16),
+            vmem(tok, BF16),
+            vmem((PART, BLOCK), BF16),
+            vmem((8, DIM), F32),
+            vmem((NY * NI, DIM), F32),
         ),
         in_specs=[pl.BlockSpec(memory_space=pl.ANY)] * 6,
-        out_specs=[pl.BlockSpec(memory_space=pl.ANY)] * 5,
+        out_specs=[pl.BlockSpec(memory_space=pltpu.VMEM)] * 5,
         scratch_shapes=[
             vmem(tok, BF16), vmem(tok, BF16), vmem(tok, BF16),
             vmem((PART, BLOCK), BF16), vmem((1, BLOCK), F32), vmem((1, WIDTH), F32),
@@ -602,29 +612,28 @@
             vmem((NZ, PART, BLOCK), BF16), vmem((BLOCK, BLOCK), BF16), vmem((BLOCK, DIM), F32),
             vmem((NZ, PART, BLOCK), BF16), vmem((4, PART, BLOCK), BF16),
             vmem((2, PART, BLOCK), BF16), vmem((2, PART // 2, BLOCK), BF16),
-            vmem((PART, BLOCK), BF16), vmem((PART, BLOCK), BF16), vmem((PART, BLOCK), BF16),
-            vmem((PART, BLOCK), F32),
+            vmem((PART, BLOCK), BF16), vmem((PART // 2, BLOCK), BF16),
             vmem((NZ, 8, DIM), F32), vmem((NZ, 8, DIM), F32), vmem((8, BLOCK), F32),
-            vmem((8, DIM), F32), vmem((8, DIM), F32),
+            vmem((8, DIM), F32),
             vmem((8, DIM), F32), vmem((NZ, 8, DIM), F32), vmem((8, DIM), F32), vmem((NI, 8, DIM), F32),
-            vmem((NI, DIM), F32), vmem((NY, NI, DIM), F32), vmem((NY * NI, DIM), F32),
+            vmem((NI, DIM), F32), vmem((NY, NI, DIM), F32),
             vmem(tok, F32), vmem(tok, F32), vmem(tok, F32),
             vmem((ROWS, DIM), F32), vmem((ROWS, DIM), F32), vmem((8, DIM), F32),
-            dma((6,)), dma((5,)),
-            dma(()), dma((NI,)), dma(()), dma(()), dma(()), dma(()), dma(()), dma(()),
+            dma((6,)),
+            dma(()), dma((NI,)), dma(()), dma(()), dma(()), dma(()), dma(()), dma((NX,)),
             dma((2,)), dma((2,)), dma(()), dma((9,)),
             dma(()), dma((NX,)), dma(()), dma((NI,)), dma(()), dma((NI,)), dma(()), dma((NI,)),
-            dma(()), dma((8,)), dma(()), dma(()), dma((4,)), dma((4,)),
+            dma(()), dma((8,)), dma(()), dma(()), dma((5,)), dma((5,)),
             dma((3,)), dma((3,)),
         ],
         compiler_params=pltpu.CompilerParams(
-            collective_id=0, has_side_effects=True, vmem_limit_bytes=67043328
+            collective_id=0, has_side_effects=True, vmem_limit_bytes=58 * 2**20
         ),
     )(
         cotangent[0], up_pre[0], value_pre[0], spatial_weight[0], spatial_bias, value_gain[None]
     )
     up_grad, value_grad, weight_grad, bias_grad, gain_grad = out
-    return up_grad[None], value_grad[None], weight_grad[None], bias_grad[:1], gain_grad.reshape(WIDTH)
+    return up_grad[None], value_grad[None], weight_grad[None].astype(F32), bias_grad[:1], gain_grad.reshape(WIDTH)
 
 
 def solution(mesh):

time: 142 us -> 129 us (0.908)
  the two profiles are of different devices: /device:TPU:69 before, /device:TPU:33 now
where the time goes in v4:
time: 129 us; the launch traced here: 128 us
  Pallas kernels  123 us (95%)
  local copies, waits for them, and re-layouts  3.76 us (3%)
    pallas_call x1, Pallas kernels, shards(): pl.pallas_call(kernel, name='gating_backward', out_shape=(vmem(tok, BF16)...  123 us
    unnamed x3, local copies, waits for them, and re-layouts  3.25 us

profile of v4, /device:TPU:33, one launch (start us, length us, event | category | flops | bytes accessed | tf_op | source)
XLA Modules:
  0.0 128.5 jit_solution(586471839495992599)
XLA Ops:
  0.6 123.3 %gating_backward.1 = (bf16[256,4096]{1,0:T(8,128)(2,1)S(1)}, bf16[256,4096]{1,0:T(8,128)(2,1)S(1)}, bf16[128,1024]{1,0:T(8,128)(2,1)S(1)}, f32[8,128]{1,0:T(8,128)S(1)}, f32[32,128]{1,0:T(8,128)S(1)}) custom-call(bf16[256,4096]{1,0:T(8,128)(2,1)} %bitcast.14, bf16[256,4096]{1,0:T(8,128)(2,1)} %bitcast.15, bf16[256,4096]{1,0:T(8,128)(2,1)} %bitcast.16, ...), custom_call_target="tpu_custom_call" | custom-call | tf_op jit(solution)/shard_map/gating_backward/pallas_call | solution.py:589
  123.9 1.3 %copy.14 = bf16[1,256,4096]{2,1,0:T(8,128)(2,1)} copy(bf16[1,256,4096]{2,1,0:T(8,128)(2,1)S(1)} %bitcast.12) | data formatting | bytes 4194304
  125.2 1.3 %copy.15 = bf16[1,256,4096]{2,1,0:T(8,128)(2,1)} copy(bf16[1,256,4096]{2,1,0:T(8,128)(2,1)S(1)} %bitcast.11) | data formatting | bytes 4194304
  126.5 0.5 slice.3
  127.0 0.6 copy.16
  127.7 0.8 bitcast_convert_fusion

commit v5 on v4

--- a/solution.py
+++ b/solution.py
@@ -196,10 +196,19 @@
         for k, (src, dst) in enumerate(moves):
             pltpu.make_async_copy(src, dst, sw_recv.at[k]).start()
 
-    for dy in range(1, NY):
-        to = lax.rem(y + dy, NY)
-        remote(S.at[1, :, to], V.at[:, span(y, ROWS)], vy_send, vy_recv, {"sp_1": to}).start()
-    pltpu.make_async_copy(S.at[1, :, y], V.at[:, span(y, ROWS)], vy_recv).start()
+    def of_chip(dx):
+        return pl.ds(lax.rem(x + dx, NX) * NC, NC)
+
+    for dx in (1, 3, 2, 0):
+        for dy in range(1, NY):
+            to = lax.rem(y + dy, NY)
+            remote(
+                S.at[1, of_chip(dx), to], V.at[of_chip(dx), span(y, ROWS)],
+                vy_send, vy_recv.at[dx], {"sp_1": to},
+            ).start()
+        pltpu.make_async_copy(
+            S.at[1, of_chip(dx), y], V.at[of_chip(dx), span(y, ROWS)], vy_recv.at[dx]
+        ).start()
 
     loads[0].wait()
     loads[1].wait()
@@ -236,14 +245,17 @@
 
     slopes(val, sv)
 
-    wait(V, vy_recv)
-    for n, d in enumerate(ORDER):
-        xi, ci = at_xc(*d)
-        dst = Y.at[1, :, span(me, DIM)]
-        if n == 0:
-            pltpu.make_async_copy(V.at[me], dst, vx_recv.at[d[0]]).start()
-        else:
-            remote(V.at[xi * NC + ci], dst, vx_send, vx_recv.at[d[0]], {"dp_0": xi, "dp_1": ci}).start()
+    for dx in (1, 3, 2, 0):
+        wait(V.at[of_chip(dx)], vy_recv.at[dx])
+        for dc in range(NC):
+            xi, ci = at_xc(dx, dc)
+            dst = Y.at[1, :, span(me, DIM)]
+            if dx + dc == 0:
+                pltpu.make_async_copy(V.at[me], dst, vx_recv.at[0]).start()
+            else:
+                remote(
+                    V.at[xi * NC + ci], dst, vx_send, vx_recv.at[dx], {"dp_0": xi, "dp_1": ci}
+                ).start()
     for n in (2, 3, 4, 5):
         relay(n)
     forward(0)
@@ -371,6 +383,8 @@
     back(2)
     outer(6, 1)
     outer(7, 0)
+    for k, dz in enumerate((1, 7)):
+        remote(ws.at[part_of(dz)], wr.at[k], gr_send, gr_recv.at[4 + k], {"sp_0": along(dz)}).start()
 
     ones = jnp.ones((8, NI * DIM), BF16)
     bsum[...] = lax.dot_general(ones, Y[0], NT, preferred_element_type=F32)
@@ -410,9 +424,6 @@
         ws[to, rows] = (ws[to, rows].astype(F32) + far4[k].astype(F32)).astype(BF16)
         remote(ws.at[to], wr.at[2 + k], gr_send, gr_recv.at[6 + k], {"sp_0": along(dz)}).start()
 
-    for k, dz in enumerate((1, 7)):
-        remote(ws.at[part_of(dz)], wr.at[k], gr_send, gr_recv.at[4 + k], {"sp_0": along(dz)}).start()
-
     for dx in (3, 1):
         for dc in range(NC):
             settle(ORDER.index((dx, dc)))
@@ -482,16 +493,17 @@
         wsum[rows, :] = total.astype(BF16)
 
     bsum[:, :DIM] = jnp.sum(br[...], axis=0)
-    first = ((wsum.at[low], wmid), (bsum.at[:, pl.ds(0, DIM)], bmid))
-    second = ((wmid, wout.at[low]), (bmid, bout))
+    some, rest = low, high
+    first = ((wsum.at[some], wmid), (bsum.at[:, pl.ds(0, DIM)], bmid))
+    second = ((wmid, wout.at[some]), (bmid, bout))
 
     @pl.when(jnp.logical_not(stays))
     def _():
-        remote(wsum.at[high], wout.at[high], so_send.at[4], so_recv.at[4], swap_from).start()
+        remote(wsum.at[rest], wout.at[rest], so_send.at[4], so_recv.at[4], swap_from).start()
 
     @pl.when(stays)
     def _():
-        pltpu.make_async_copy(wsum.at[high], wout.at[high], so_recv.at[4]).start()
+        pltpu.make_async_copy(wsum.at[rest], wout.at[rest], so_recv.at[4]).start()
 
     @pl.when(mine != me)
     def _():
@@ -508,6 +520,10 @@
         row_sums(n)
     for n in (2, 3, 4, 5):
         finish(n)
+    for n in (1, 0):
+        row_sums(n)
+    for n in (1, 0):
+        finish(n)
     for n in (6, 7):
         row_sums(n)
     finish_gain()
@@ -525,8 +541,6 @@
         for k, (src, dst) in enumerate(second):
             pltpu.make_async_copy(src, dst, so_recv.at[2 + k]).start()
 
-    for n in (1, 0):
-        row_sums(n)
 
     @pl.loop(0, ROWS // 16)
     def _(t):
@@ -540,15 +554,15 @@
             grad = (scale * scaled - cube * act[rows, at]) * sv[rows, at]
             valg[rows, at] = grad.astype(BF16)
 
-    for n in (6, 7, 1, 0):
+    for n in (6, 7):
         finish(n)
 
     wait(gy, gn_recv.at[2])
     for i in range(NI):
         for k in range(NY):
             gall[i * NY + k : i * NY + k + 1, :] = gy[k, i : i + 1, :]
-    wait(wout.at[low], so_recv.at[2])
-    wait(wout.at[high], so_recv.at[4])
+    wait(wout.at[some], so_recv.at[2])
+    wait(wout.at[rest], so_recv.at[4])
     wait(bout, so_recv.at[3])
 
     wait(X.at[pl.ds(0, NI - 1)], xo_send)
@@ -570,7 +584,7 @@
     def _():
         for k, (src, dst) in enumerate(moves):
             wait(src, sw_send.at[k])
-        wait(wsum.at[high], so_send.at[4])
+        wait(wsum.at[rest], so_send.at[4])
 
     @pl.when(mine != me)
     def _():
@@ -620,7 +634,7 @@
             vmem(tok, F32), vmem(tok, F32), vmem(tok, F32),
             vmem((ROWS, DIM), F32), vmem((ROWS, DIM), F32), vmem((8, DIM), F32),
             dma((6,)),
-            dma(()), dma((NI,)), dma(()), dma(()), dma(()), dma(()), dma(()), dma((NX,)),
+            dma(()), dma((NI,)), dma(()), dma(()), dma(()), dma((NX,)), dma(()), dma((NX,)),
             dma((2,)), dma((2,)), dma(()), dma((9,)),
             dma(()), dma((NX,)), dma(()), dma((NI,)), dma(()), dma((NI,)), dma(()), dma((NI,)),
             dma(()), dma((8,)), dma(()), dma(()), dma((5,)), dma((5,)),

time: 129 us -> 129 us (level)
  no operation moved by 1% of the time
where the time goes in v5:
time: 129 us
  Pallas kernels  123 us (95%)
  local copies, waits for them, and re-layouts  3.76 us (3%)
    pallas_call x1, Pallas kernels, shards(): pl.pallas_call(kernel, name='gating_backward', out_shape=(vmem(tok, BF16)...  123 us
    unnamed x3, local copies, waits for them, and re-layouts  3.25 us

profile of v5, /device:TPU:33, one launch (start us, length us, event | category | flops | bytes accessed | tf_op | source)
XLA Modules:
  0.0 128.6 jit_solution(13425239046933045055)
XLA Ops:
  0.6 123.4 %gating_backward.1 = (bf16[256,4096]{1,0:T(8,128)(2,1)S(1)}, bf16[256,4096]{1,0:T(8,128)(2,1)S(1)}, bf16[128,1024]{1,0:T(8,128)(2,1)S(1)}, f32[8,128]{1,0:T(8,128)S(1)}, f32[32,128]{1,0:T(8,128)S(1)}) custom-call(bf16[256,4096]{1,0:T(8,128)(2,1)} %bitcast.14, bf16[256,4096]{1,0:T(8,128)(2,1)} %bitcast.15, bf16[256,4096]{1,0:T(8,128)(2,1)} %bitcast.16, ...), custom_call_target="tpu_custom_call" | custom-call | tf_op jit(solution)/shard_map/gating_backward/pallas_call | solution.py:603
  124.0 1.3 %copy.14 = bf16[1,256,4096]{2,1,0:T(8,128)(2,1)} copy(bf16[1,256,4096]{2,1,0:T(8,128)(2,1)S(1)} %bitcast.12) | data formatting | bytes 4194304
  125.4 1.3 %copy.15 = bf16[1,256,4096]{2,1,0:T(8,128)(2,1)} copy(bf16[1,256,4096]{2,1,0:T(8,128)(2,1)S(1)} %bitcast.11) | data formatting | bytes 4194304
  126.7 0.5 slice.3
  127.2 0.6 copy.16
  127.8 0.8 bitcast_convert_fusion
